TPU v7x, 32 devices: a whole 2x2x4 slice. The times are simulated.
32 devices in a mesh: sp: 8 (over z, x), tp: 4 (over y, core).
Axes of the slice: x: 2, y: 2, z: 4, core: 2. Of those that a mesh axis runs over, the one named last changes fastest.
Arguments:
- residual: bfloat16 [4096, 2048], P(('sp', 'tp')), may hold values from -6 to 6
- query_small: bfloat16 [4096, 8, 128], P('sp', 'tp'), may hold values from -120 to 120
- key_small: bfloat16 [4096, 8, 128], P('sp', 'tp'), may hold values from -6 to 6
- value_small: bfloat16 [4096, 8, 128], P('sp', 'tp'), may hold values from -6 to 6
- query_large: bfloat16 [4096, 8, 256], P('sp', 'tp'), may hold values from -120 to 120
- key_large: bfloat16 [4096, 8, 256], P('sp', 'tp'), may hold values from -6 to 6
- value_large: bfloat16 [4096, 8, 128], P('sp', 'tp'), may hold values from -6 to 6
- lambda_small: float32 [8], P('tp'), may hold values from 0.3 to 0.8
- lambda_large: float32 [8], P('tp'), may hold values from 0.3 to 0.8
- head_gain: float32 [128], replicated, may hold values from 0.1 to 1.9
- output_small: bfloat16 [1024, 2048], P('tp'), may hold values from -0.125 to 0.125
- output_large: bfloat16 [1024, 2048], P('tp'), may hold values from -0.125 to 0.125
- norm_gain: float32 [2048], replicated, may hold values from 0.1 to 1.9
- gate_weight: bfloat16 [2048, 5632], P('sp', 'tp'), may hold values from -0.125 to 0.125
- up_weight: bfloat16 [2048, 5632], P('sp', 'tp'), may hold values from -0.125 to 0.125
- down_weight: bfloat16 [5632, 2048], P('tp', 'sp'), may hold values from -0.3125 to 0.3125
Outputs:
- block_output: bfloat16 [4096, 2048], P(('sp', 'tp'))
All inputs are finite; a program needn't handle non-finite values.
Results may differ from a plain program's by a relative error of at most 0.015.
Values may be sent and summed in bfloat16 or wider, within the bound.
A program may use at most 128 MiB of HBM per device.

v0:
```python
import functools

import jax
import jax.numpy as jnp
from jax import lax
from jax.experimental import pallas as pl
from jax.experimental.pallas import tpu as pltpu
from jax.sharding import PartitionSpec as P

residual_scale = 8.0**0.25
branch_scale = 0.8
norm_epsilon = 1e-05
masked_score = -1e30
log2_e = 1.4426950408889634
MESH = pl.DeviceIdType.MESH


def layer_norm(values, gains):
    centered = values - jnp.mean(values, axis=-1, keepdims=True)
    variance = jnp.mean(centered * centered, axis=-1, keepdims=True)
    return centered * lax.rsqrt(variance + norm_epsilon) * gains


def fold_lanes(values, op):
    result = values[:, :128]
    for start in range(128, values.shape[1], 128):
        result = op(result, values[:, start : start + 128])
    return result


class Plan:
    def __init__(self, n, m, small, large, tokens, rows, small_size, large_size):
        self.n, self.m = n, m
        self.slots = small + large
        self.group = n // self.slots
        half = small // 2
        self.kinds = [("s", i) for i in range(half)]
        self.kinds += [("l", i) for i in range(large)]
        self.kinds += [("s", i) for i in range(half, small)]
        self.keys = [1 if kind == "s" else 2 for kind, _ in self.kinds]
        self.starts = []
        at = 0
        for k in self.keys:
            self.starts.append(at)
            at += 2 * k + 1
        self.tokens, self.rows = tokens, rows
        self.small_size, self.large_size = small_size, large_size
        order = []
        lo, hi = 0, self.slots - 1
        while lo <= hi:
            order.append(hi)
            if lo < hi:
                order.append(lo)
            lo, hi = lo + 1, hi - 1
        self.order = order


def attend_kernel(plan, lam_ref, planes, gain_ref, att_ref, kv, q, o, att, peak, total, acc,
                  kvz_s, kvz_r, qz_s, qz_r, kvx_s, kvx_r, loc, o_s, o_r, o_l):
    slots, group, m = plan.slots, plan.group, plan.m
    tokens, rows = plan.tokens, plan.rows
    s = lax.axis_index("sp")
    t = lax.axis_index("tp")
    a, b = s // group, s % group
    aside = lax.rem(s + 1, plan.n)
    mine = pl.ds(pl.multiple_of(s * tokens, tokens), tokens)
    large = a < 0
    for i, k in enumerate(plan.keys):
        if k == 2:
            large = jnp.logical_or(large, a == i)
    by_kind = ((1, jnp.logical_not(large)), (2, large))

    def kv_z(i, to):
        k = plan.keys[i]
        return pltpu.make_async_remote_copy(
            src_ref=planes.at[pl.ds(plan.starts[i], k + 1)],
            dst_ref=kv.at[pl.ds(0, k + 1), mine],
            send_sem=kvz_s.at[i], recv_sem=kvz_r.at[a],
            device_id={"sp": to * group + b, "tp": t}, device_id_type=MESH)

    def q_z(i, to):
        k = plan.keys[i]
        return pltpu.make_async_remote_copy(
            src_ref=planes.at[pl.ds(plan.starts[i] + k + 1, k)],
            dst_ref=q.at[pl.ds(0, k), a],
            send_sem=qz_s.at[i], recv_sem=qz_r.at[a],
            device_id={"sp": to * group + b, "tp": t}, device_id_type=MESH)

    def kv_own(i):
        k = plan.keys[i]
        return pltpu.make_async_copy(
            planes.at[pl.ds(plan.starts[i], k + 1)], kv.at[pl.ds(0, k + 1), mine], loc.at[0])

    def q_own(i):
        k = plan.keys[i]
        return pltpu.make_async_copy(
            planes.at[pl.ds(plan.starts[i] + k + 1, k)], q.at[pl.ds(0, k), a], loc.at[1])

    def peer(j):
        return a * group + lax.rem(b + j, group)

    def kv_x(k, i, j):
        block = pl.ds(pl.multiple_of((i * group + b) * tokens, tokens), tokens)
        return pltpu.make_async_remote_copy(
            src_ref=kv.at[pl.ds(0, k + 1), block],
            dst_ref=kv.at[pl.ds(0, k + 1), block],
            send_sem=kvx_s.at[i, j - 1], recv_sem=kvx_r.at[i, j - 1],
            device_id={"sp": peer(j), "tp": t}, device_id_type=MESH)

    for i in range(slots):
        @pl.when(a == i)
        def _():
            kv_own(i).start()
            q_own(i).start()

    for i in plan.order:
        @pl.when(a != i)
        def _():
            kv_z(i, i).start()
    for i in plan.order:
        @pl.when(a != i)
        def _():
            q_z(i, i).start()

    for i in range(slots):
        @pl.when(a == i)
        def _():
            kv_own(i).wait()
            q_own(i).wait()

    for j in range(1, group):
        for i in range(slots):
            @pl.when(a == i)
            def _():
                kv_x(plan.keys[i], i, j).start()

    for distance in range(1, slots):
        for i in range(slots):
            @pl.when(jnp.abs(a - i) == distance)
            def _():
                for k, when in by_kind:
                    @pl.when(when)
                    def _():
                        source = pl.ds(pl.multiple_of((i * group + b) * tokens, tokens), tokens)
                        pltpu.make_async_remote_copy(
                            src_ref=kv.at[pl.ds(0, k + 1), source],
                            dst_ref=kv.at[pl.ds(0, k + 1), source],
                            send_sem=kvz_s.at[i], recv_sem=kvz_r.at[i],
                            device_id={"sp": aside, "tp": t}, device_id_type=MESH).wait_recv()
                        for j in range(1, group):
                            kv_x(k, i, j).start()

    for i in range(slots):
        for k, when in by_kind:
            @pl.when(when)
            def _():
                @pl.when(a != i)
                def _():
                    pltpu.make_async_remote_copy(
                        src_ref=q.at[pl.ds(0, k), i], dst_ref=q.at[pl.ds(0, k), i],
                        send_sem=qz_s.at[i], recv_sem=qz_r.at[i],
                        device_id={"sp": aside, "tp": t}, device_id_type=MESH).wait_recv()

                for j in range(1, group):
                    kv_x(k, i, j).wait_recv()

    @pl.when(jnp.logical_not(large))
    def _():
        for i in range(slots):
            both = q[0, i]
            lane = lax.broadcasted_iota(jnp.int32, both.shape, 1)
            q[1, i] = jnp.where(lane >= plan.small_size, both, jnp.zeros_like(both))
            q[0, i] = jnp.where(lane < plan.small_size, both, jnp.zeros_like(both))

    lift = large.astype(jnp.int32)
    factor = jnp.where(large, plan.large_size**-0.5 * log2_e, plan.small_size**-0.5 * log2_e)
    lam = lam_ref[a]
    last = (((1,), (1,)), ((), ()))
    high = min(256, tokens)
    parts = tokens // high
    owners = high // rows
    head = t * slots + a

    def o_copy(i, part, w):
        which = part * owners + w
        return pltpu.make_async_remote_copy(
            src_ref=o.at[i, pl.ds(pl.multiple_of(which * rows, rows), rows)],
            dst_ref=att.at[head],
            send_sem=o_s.at[i, which], recv_sem=o_r.at[head],
            device_id={"sp": i * group + b, "tp": which}, device_id_type=MESH)

    def attend(step, carry):
        i, part = step // parts, lax.rem(step, parts)
        block = i * group + b
        row0 = part * high
        here = pl.ds(pl.multiple_of(row0, high), high)
        queries = (q[0, i, here], q[1, i, here])

        def score(which, start):
            keys = kv[which * lift, pl.ds(pl.multiple_of(start, tokens), tokens)]
            return lax.dot_general(queries[which], keys, last, preferred_element_type=jnp.float32)

        def masked(which):
            near = score(which, block * tokens)
            row = row0 + lax.broadcasted_iota(jnp.int32, near.shape, 0)
            column = lax.broadcasted_iota(jnp.int32, near.shape, 1)
            return jnp.where(column <= row, near, masked_score)

        for which in range(2):
            peak[which] = fold_lanes(masked(which), jnp.maximum)

        def find(c, carry):
            for which in range(2):
                peak[which] = jnp.maximum(
                    peak[which], fold_lanes(score(which, c * tokens), jnp.maximum))
            return carry

        lax.fori_loop(0, block, find, 0)
        tops = [jnp.max(peak[which], axis=1, keepdims=True) for which in range(2)]
        for which in range(2):
            peak[which] = jnp.broadcast_to(tops[which], (high, 128))

        def weigh(which, values, start, first):
            top = peak[which][:, :1]
            weights = jnp.exp2((values - top) * factor)
            value = kv[1 + lift, pl.ds(pl.multiple_of(start, tokens), tokens)]
            part_sum = fold_lanes(weights, jnp.add)
            part_acc = jnp.dot(weights.astype(jnp.bfloat16), value, preferred_element_type=jnp.float32)
            if first:
                total[which] = part_sum
                acc[which] = part_acc
            else:
                total[which] += part_sum
                acc[which] += part_acc

        for which in range(2):
            weigh(which, masked(which), block * tokens, True)

        def far(c, carry):
            for which in range(2):
                weigh(which, score(which, c * tokens), c * tokens, False)
            return carry

        lax.fori_loop(0, block, far, 0)
        outs = [acc[which] / jnp.sum(total[which], axis=1, keepdims=True) for which in range(2)]
        combined = outs[0] - lam * outs[1]
        mean_square = jnp.mean(combined * combined, axis=1, keepdims=True)
        normed = combined * lax.rsqrt(mean_square + norm_epsilon) * gain_ref[...] * branch_scale
        o[i, here] = normed.astype(o.dtype)
        return carry

    def send(step, carry):
        i, part = step // parts, lax.rem(step, parts)
        for w in range(owners):
            self_here = jnp.logical_and(i == a, part * owners + w == t)

            @pl.when(jnp.logical_not(self_here))
            def _():
                o_copy(i, part, w).start()
        return carry

    steps = slots * parts

    def step_body(step, carry):
        attend(step, carry)

        @pl.when(step > 0)
        def _():
            send(step - 1, carry)

        return carry

    lax.fori_loop(0, steps, step_body, 0)
    att[head] = o[a, pl.ds(pl.multiple_of(t * rows, rows), rows)]
    send(steps - 1, 0)

    for h in range(m * slots):
        @pl.when(head != h)
        def _():
            pltpu.make_async_remote_copy(
                src_ref=att.at[h], dst_ref=att.at[h], send_sem=o_s.at[0, 0], recv_sem=o_r.at[h],
                device_id={"sp": aside, "tp": t}, device_id_type=MESH).wait_recv()
    att_ref[...] = att[...]

    for i in range(slots):
        @pl.when(a != i)
        def _():
            kv_z(i, i).wait_send()
            q_z(i, i).wait_send()

        for k, when in by_kind:
            @pl.when(when)
            def _():
                for j in range(1, group):
                    kv_x(k, i, j).wait_send()
        for part in range(parts):
            for w in range(owners):
                @pl.when(jnp.logical_not(jnp.logical_and(i == a, part * owners + w == t)))
                def _():
                    o_copy(i, part, w).wait_send()


def attend(plan, lams, planes, gain, width):
    dma = pltpu.SemaphoreType.DMA
    slots, n, m = plan.slots, plan.n, plan.m
    high = min(256, plan.tokens)
    any_space = pl.BlockSpec(memory_space=pl.ANY)
    vmem = pl.BlockSpec(memory_space=pltpu.VMEM)
    others = max(plan.group - 1, 1)
    return pl.pallas_call(
        functools.partial(attend_kernel, plan),
        out_shape=jax.ShapeDtypeStruct((m * slots, plan.rows, width), jnp.bfloat16),
        in_specs=[pl.BlockSpec(memory_space=pltpu.SMEM), any_space, vmem],
        out_specs=vmem,
        scratch_shapes=[
            pltpu.VMEM((3, n * plan.tokens, width), jnp.bfloat16),
            pltpu.VMEM((2, slots, plan.tokens, width), jnp.bfloat16),
            pltpu.VMEM((slots, plan.tokens, width), jnp.bfloat16),
            pltpu.VMEM((m * slots, plan.rows, width), jnp.bfloat16),
            pltpu.VMEM((2, high, 128), jnp.float32),
            pltpu.VMEM((2, high, 128), jnp.float32),
            pltpu.VMEM((2, high, width), jnp.float32),
            dma((slots,)), dma((slots,)), dma((slots,)), dma((slots,)),
            dma((slots, others)), dma((slots, others)),
            dma((2,)),
            dma((slots, plan.tokens // plan.rows)), dma((m * slots,)), dma,
        ],
        compiler_params=pltpu.CompilerParams(
            vmem_limit_bytes=60 * 2**20, has_side_effects=True),
        cost_estimate=pl.CostEstimate(
            flops=60_000_000_000, bytes_accessed=planes.size * 2, transcendentals=8_000_000),
        name="attend",
    )(lams, planes, gain.reshape(1, width))


def swap(value, axis, bit):
    pairs = [(i, i ^ (1 << bit)) for i in range(lax.axis_size(axis))]
    return lax.ppermute(value, axis, pairs)


def gather_rows(rows, bits):
    held = {0: rows}
    for bit in reversed(range(bits)):
        keys = sorted(held)
        sent = jnp.concatenate([held[k] for k in keys], axis=0) if len(keys) > 1 else held[0]
        got = swap(sent, "tp", bit)
        for i, k in enumerate(keys):
            held[k | (1 << bit)] = got[i * rows.shape[0] : (i + 1) * rows.shape[0]]
    return jnp.concatenate([held[k] for k in sorted(held)], axis=0)


def scatter_sum(values, bits):
    rows = values.shape[0] >> bits
    held = {k: values[k * rows : (k + 1) * rows] for k in range(1 << bits)}
    for bit in range(bits):
        kept = [k for k in sorted(held) if not k >> bit & 1]
        sent = [held[k | (1 << bit)].astype(jnp.bfloat16) for k in kept]
        got = swap(jnp.concatenate(sent, axis=0) if len(sent) > 1 else sent[0], "tp", bit)
        held = {
            k: held[k] + got[i * rows : (i + 1) * rows].astype(jnp.float32)
            for i, k in enumerate(kept)
        }
    return held[0]


def per_device(
    residual, query_small, key_small, value_small, query_large, key_large, value_large,
    lambda_small, lambda_large, head_gain, output_small, output_large, norm_gain,
    gate_weight, up_weight, down_weight,
):
    tokens, heads_small, width = value_small.shape
    heads_large = value_large.shape[1]
    rows, _ = residual.shape
    n, m = lax.axis_size("sp"), lax.axis_size("tp")
    bits = m.bit_length() - 1
    plan = Plan(n, m, heads_small, heads_large, tokens, rows,
                query_small.shape[2] // 2, query_large.shape[2] // 2)
    half = plan.large_size
    planes, lams, weights = [], [], []
    for kind, i in plan.kinds:
        if kind == "s":
            planes += [key_small[:, i], value_small[:, i], query_small[:, i]]
            lams.append(lambda_small[i])
            weights.append(output_small[i * width : (i + 1) * width])
        else:
            planes += [key_large[:, i, :half], key_large[:, i, half:], value_large[:, i],
                       query_large[:, i, :half], query_large[:, i, half:]]
            lams.append(lambda_large[i])
            weights.append(output_large[i * width : (i + 1) * width])
    output_full = lax.all_gather(jnp.concatenate(weights, axis=0), "tp", axis=0, tiled=True)
    gate_full = lax.all_gather(gate_weight, "sp", axis=0, tiled=True)
    up_full = lax.all_gather(up_weight, "sp", axis=0, tiled=True)
    down_full = lax.all_gather(down_weight, "sp", axis=1, tiled=True)
    attended = attend(plan, jnp.stack(lams), jnp.stack(planes), head_gain, width)
    attended = jnp.transpose(attended, (1, 0, 2)).reshape(rows, -1)
    mixed_sum = jnp.dot(attended, output_full, preferred_element_type=jnp.float32)
    normed = layer_norm(
        residual_scale * residual.astype(jnp.float32) + mixed_sum, norm_gain
    ).astype(jnp.bfloat16)
    whole_rows = gather_rows(normed, bits)
    gate_rows = jnp.dot(whole_rows, gate_full, preferred_element_type=jnp.float32)
    up_rows = jnp.dot(whole_rows, up_full, preferred_element_type=jnp.float32)
    hidden = (jax.nn.silu(gate_rows) * up_rows).astype(jnp.bfloat16)
    down_sum = scatter_sum(
        jnp.dot(hidden, down_full, preferred_element_type=jnp.float32), bits
    )
    return (residual_scale * normed.astype(jnp.float32) + 0.5 * down_sum).astype(jnp.bfloat16)


def solution(mesh):
    in_specs = (
        P(("sp", "tp"), None), P("sp", "tp", None), P("sp", "tp", None), P("sp", "tp", None),
        P("sp", "tp", None), P("sp", "tp", None), P("sp", "tp", None), P("tp"), P("tp"), P(),
        P("tp", None), P("tp", None), P(), P("sp", "tp"), P("sp", "tp"), P("tp", "sp"),
    )

    return jax.shard_map(
        per_device, mesh=mesh, in_specs=in_specs, out_specs=P(("sp", "tp"), None), check_vma=False
    )
```

profile of v0, /device:TPU:0, one launch (start us, length us, event | category | flops | bytes accessed | tf_op | source)
XLA Modules:
  0.0 402.8 jit_solution(13253385178101442083)
XLA Ops:
  6.5 1.4 fusion.31
  8.1 1.4 pad_maximum_fusion
  9.6 0.7 all-gather.9.cloned.1.call-update
  10.4 0.7 all-gather.11.cloned.1.call-update
  11.1 0.5 all-gather.7.cloned.1.call-update
  11.7 0.4 fusion.36
  12.1 0.4 fusion.35
  12.5 0.4 fusion.34
  12.9 0.7 fusion.33
  13.6 0.4 fusion.37
  14.0 0.7 fusion.32
  14.8 0.6 fusion.38
  16.0 0.2 copy-done.12
  16.2 1.9 pad_maximum_fusion.10.lam_ref
  18.1 93.1 %attend.1 = bf16[16,128,128]{2,1,0:T(8,128)(2,1)} custom-call(f32[4]{0:T(128)} %pad_maximum_fusion.10.lam_ref, bf16[16,512,128]{2,1,0:T(8,128)(2,1)} %copy-done.10, f32[1,128]{1,0:T(1,128)} %bitcast.74), custom_call_target="tpu_custom_call" | custom-call | flops 60000002048 | bytes 2097152 | tf_op jit(solution)/shard_map/attend/pallas_call | solution.py:310
  111.2 1.3 copy.49
  112.6 4.8 %fusion.39 = (f32[128]{0:T(128)S(1)}, f32[128,2048]{1,0:T(8,128)S(1)}) fusion(bf16[128,2048]{0,1:T(8,128)(2,1)S(1)} %bitcast.72, bf16[2048,2048]{1,0:T(8,128)(2,1)} %all-gather.5.cloned.1.call-done, bf16[128,2048]{1,0:T(8,128)(2,1)S(1)} %copy-done.8), kind=kOutput, calls=%fused_computation.67 | convolution fusion | flops 1074790272 | bytes 10486272 | tf_op jit(solution)/shard_map/dot_general | solution.py:396
  117.4 0.3 multiply_reduce_fusion
  117.9 5.4 %collective-permute-start = (bf16[128,2048]{1,0:T(8,128)(2,1)S(1)}, bf16[128,2048]{1,0:T(8,128)(2,1)S(1)}, u32[]{:S(2)}, u32[]{:S(2)}) collective-permute-start(bf16[128,2048]{1,0:T(8,128)(2,1)S(1)} %multiply_convert_fusion.2), channel_id=1, source_target_pairs={{0,2},{1,3},{2,0},{3,1},{4,6},{5,7},{6,4},{7,5},{8,10},{9,11},{10,... | collective-permute-start | bytes 1572872 | tf_op jit(solution)/shard_map/ppermute | solution.py:338
  123.2 12.0 %collective-permute-done = bf16[128,2048]{1,0:T(8,128)(2,1)S(1)} collective-permute-done((bf16[128,2048]{1,0:T(8,128)(2,1)S(1)}, bf16[128,2048]{1,0:T(8,128)(2,1)S(1)}, u32[]{:S(2)}, u32[]{:S(2)}) %collective-permute-start) | collective-permute-done | bytes 524320 | tf_op jit(solution)/shard_map/ppermute | solution.py:338
  135.4 1.0 collective-permute-start.1
  136.4 2.3 collective-permute-done.1
  138.8 35.9 %all-gather.9.cloned.1.call-done = bf16[2048,1408]{1,0:T(8,128)(2,1)} async-done(((bf16[256,1408]{1,0:T(8,128)(2,1)}), bf16[2048,1408]{1,0:T(8,128)(2,1)}) %all-gather.9.cloned.1.call-update) | async-done | bytes 5767184 | tf_op jit(solution)/shard_map/all_gather | solution.py:392
  174.7 7.7 %fusion.7 = f32[512,1408]{1,0:T(8,128)} fusion(bf16[2048,1408]{1,0:T(8,128)(2,1)} %all-gather.9.cloned.1.call-done, bf16[128,2048]{1,0:T(8,128)(2,1)S(1)} %get-tuple-element.8, bf16[128,2048]{1,0:T(8,128)(2,1)S(1)} %collective-permute-done, bf16[128,2048]{1,0:T(8,128)(2,1)S(1)} %get-tuple-element.7, bf16[128,2048]{1,0:T(8,128)(2,1)S(1)} %multiply_convert_fusion.2), kind=kOutput, calls=%fused_computation.17 | convolution fusion | flops 2961178624 | bytes 10747904 | tf_op jit(solution)/shard_map/dot_general | solution.py:402
  182.3 87.0 %all-gather.11.cloned.1.call-done = bf16[1408,2048]{1,0:T(8,128)(2,1)} async-done(((bf16[1408,256]{1,0:T(8,128)(2,1)}), bf16[1408,2048]{1,0:T(8,128)(2,1)}) %all-gather.11.cloned.1.call-update) | async-done | bytes 5767184 | tf_op jit(solution)/shard_map/all_gather | solution.py:393
  269.3 92.6 %all-gather.7.cloned.1.call-done = bf16[2048,1408]{1,0:T(8,128)(2,1)} async-done(((bf16[256,1408]{1,0:T(8,128)(2,1)}), bf16[2048,1408]{1,0:T(8,128)(2,1)}) %all-gather.7.cloned.1.call-update) | async-done | bytes 5767184 | tf_op jit(solution)/shard_map/all_gather | solution.py:391
  361.9 14.8 %fusion.40 = (bf16[512,2048]{1,0:T(8,128)(2,1)}, f32[512,2048]{1,0:T(8,128)}) fusion(bf16[1408,2048]{1,0:T(8,128)(2,1)} %all-gather.11.cloned.1.call-done, f32[512,1408]{1,0:T(8,128)} %fusion.7, bf16[2048,1408]{1,0:T(8,128)(2,1)} %all-gather.7.cloned.1.call-done, bf16[128,2048]{1,0:T(8,128)(2,1)S(1)} %get-tuple-element.8, ...), kind=kOutput, calls=%fused_computation.68 | convolution fusion | flops 5919342592 | bytes 22806528 | tf_op jit(solution)/shard_map/dot_general | solution.py:405
  376.6 1.4 fusion.29
  378.2 2.6 collective-permute-done.2
  381.0 1.5 collective-permute-start.3
  382.6 12.5 %collective-permute-done.3 = bf16[128,2048]{1,0:T(8,128)(2,1)S(1)} collective-permute-done((bf16[128,2048]{1,0:T(8,128)(2,1)S(1)}, bf16[128,2048]{1,0:T(8,128)(2,1)S(1)}, u32[]{:S(2)}, u32[]{:S(2)}) %collective-permute-start.3) | collective-permute-done | bytes 524320 | tf_op jit(solution)/shard_map/ppermute | solution.py:338
  395.0 1.3 fusion.6
  (55 shorter events, 1.5 us)
Async XLA Ops:
  6.5 1.5 copy-start.7
  6.5 106.0 %all-gather.5.cloned.1.call-start = ((), (), s32[]{:S(2)}) async-start(), calls=%async_computation | async-start | bytes 10485760 | tf_op jit(solution)/shard_map/all_gather | solution.py:390
  9.5 2.1 copy-start.2
  9.6 2.5 copy-start.3
  9.6 165.1 %all-gather.9.cloned.1.call-start = ((), (), s32[]{:S(2)}) async-start(), calls=%async_computation.2 | async-start | bytes 6488064 | tf_op jit(solution)/shard_map/all_gather | solution.py:392
  10.3 2.1 copy-start.4
  10.3 259.0 %all-gather.11.cloned.1.call-start = ((), (), s32[]{:S(2)}) async-start(), calls=%async_computation.3 | async-start | bytes 6488064 | tf_op jit(solution)/shard_map/all_gather | solution.py:393
  11.1 1.8 copy-start
  11.1 350.8 %all-gather.7.cloned.1.call-start = ((), (), s32[]{:S(2)}) async-start(), calls=%async_computation.1 | async-start | bytes 6488064 | tf_op jit(solution)/shard_map/all_gather | solution.py:391
  12.1 1.5 copy-start.5
  12.5 1.5 copy-start.1
  13.6 1.1 copy-start.11
  15.6 0.7 copy-start.12
  16.0 2.2 copy-start.10
  18.1 94.4 %copy-start.8 = (bf16[128,2048]{1,0:T(8,128)(2,1)S(1)}, bf16[128,2048]{1,0:T(8,128)(2,1)}, u32[]{:S(2)}) copy-start(bf16[128,2048]{1,0:T(8,128)(2,1)} %param.16) | copy-start | bytes 1572868
  112.6 5.1 %copy-start.9 = (f32[2048]{0:T(1024)S(1)}, f32[2048]{0:T(1024)}, u32[]{:S(2)}) copy-start(f32[2048]{0:T(1024)} %param.28) | copy-start | bytes 24580
  117.9 17.4 %collective-permute-start = (bf16[128,2048]{1,0:T(8,128)(2,1)S(1)}, bf16[128,2048]{1,0:T(8,128)(2,1)S(1)}, u32[]{:S(2)}, u32[]{:S(2)}) collective-permute-start(bf16[128,2048]{1,0:T(8,128)(2,1)S(1)} %multiply_convert_fusion.2), channel_id=1, source_target_pairs={{0,2},{1,3},{2,0},{3,1},{4,6},{5,7},{6,4},{7,5},{8,10},{9,11},{10,... | collective-permute-start | bytes 1572872 | tf_op jit(solution)/shard_map/ppermute | solution.py:338
  135.4 3.3 collective-permute-start.1
  376.6 4.3 %copy-start.6 = (f32[512,2048]{1,0:T(8,128)S(1)}, f32[512,2048]{1,0:T(8,128)}, u32[]{:S(2)}) copy-start(f32[512,2048]{1,0:T(8,128)} %get-tuple-element.32) | copy-start | bytes 12582916
  378.2 2.7 collective-permute-start.2
  381.0 14.0 %collective-permute-start.3 = (bf16[128,2048]{1,0:T(8,128)(2,1)S(1)}, bf16[128,2048]{1,0:T(8,128)(2,1)S(1)}, u32[]{:S(2)}, u32[]{:S(2)}) collective-permute-start(bf16[128,2048]{1,0:T(8,128)(2,1)S(1)} %fusion.2), channel_id=1, source_target_pairs={{0,2},{1,3},{2,0},{3,1},{4,6},{5,7},{6,4},{7,5},{8,10},{9,11},{10,... | collective-permute-start | bytes 1572872 | tf_op jit(solution)/shard_map/ppermute | solution.py:338
Sparse Core Ops, SparseCore 0:
  9.7 60.9 all-gather.4
  72.9 101.7 all-gather.8
  176.7 92.5 all-gather.10
  271.3 90.4 all-gather.6
where the time goes:
time: 403 us
  waiting for transfers between devices  247 us (61%)
  Pallas kernels  93.1 us (23%)
  matrix products  27.2 us (7%)
  between operations  13.5 us (3%)
  local copies, waits for them, and re-layouts  8.7 us (2%)
  starting transfers between devices  8.14 us (2%)
  other arithmetic  5.41 us (1%)
    pallas_call x1, Pallas kernels, attend(): pl.pallas_call(functools.partial(attend_kernel, plan), out_shape=jax.Shap...  93.1 us
    all_gather x1, waiting for transfers between devices, per_device(): gate_full = lax.all_gather(gate_weight, 'sp', axis=0, tiled=True)  92.6 us
    all_gather x1, waiting for transfers between devices, per_device(): down_full = lax.all_gather(down_weight, 'sp', axis=1, tiled=True)  87 us
    all_gather x1, waiting for transfers between devices, per_device(): up_full = lax.all_gather(up_weight, 'sp', axis=0, tiled=True)  35.9 us
    ppermute x4, waiting for transfers between devices, swap(): return lax.ppermute(value, axis, pairs)  29.5 us
    dot_general x1, matrix products, per_device(): jnp.dot(hidden, down_full, preferred_element_type=jnp.float32)  14.8 us
  transfers between devices with their start and end apart: 8, of which 7 were waited for; matrix products, arithmetic and copies ran while one was open for 5% of the time, Pallas kernels for 23%

commit v1 on v0

v1 whole, which is shorter than its diff:
```python
import functools

import jax
import jax.numpy as jnp
from jax import lax
from jax.experimental import pallas as pl
from jax.experimental.pallas import tpu as pltpu
from jax.sharding import PartitionSpec as P

residual_scale = 8.0**0.25
branch_scale = 0.8
norm_epsilon = 1e-05
masked_score = -1e30
log2_e = 1.4426950408889634
MESH = pl.DeviceIdType.MESH


def layer_norm(values, gains):
    centered = values - jnp.mean(values, axis=-1, keepdims=True)
    variance = jnp.mean(centered * centered, axis=-1, keepdims=True)
    return centered * lax.rsqrt(variance + norm_epsilon) * gains


def fold_lanes(values, op):
    result = values[:, :128]
    for start in range(128, values.shape[1], 128):
        result = op(result, values[:, start : start + 128])
    return result


class Plan:
    def __init__(self, n, m, small, large, tokens, rows, small_size, large_size):
        self.n, self.m = n, m
        self.slots = small + large
        self.group = n // self.slots
        half = small // 2
        self.kinds = [("s", i) for i in range(half)]
        self.kinds += [("l", i) for i in range(large)]
        self.kinds += [("s", i) for i in range(half, small)]
        self.keys = [1 if kind == "s" else 2 for kind, _ in self.kinds]
        self.starts = []
        at = 0
        for k in self.keys:
            self.starts.append(at)
            at += 2 * k + 1
        self.tokens, self.rows = tokens, rows
        self.small_size, self.large_size = small_size, large_size
        order = []
        lo, hi = 0, self.slots - 1
        while lo <= hi:
            order.append(hi)
            if lo < hi:
                order.append(lo)
            lo, hi = lo + 1, hi - 1
        self.order = order

    def mixer(self, features, units):
        tiles = units // 128
        first = (tiles + 1) // 2 * 128
        self.sizes, self.offsets = (first, units - first), (0, first)
        self.depth = features // self.n
        self.features = features
        self.chips = self.m // 2
        self.peers = 2 * self.chips


def layer_kernel(plan, lam_ref, planes, gain_ref, out_w, residual_ref, norm_ref, gate, up, down, out_ref,
                 kv, q, o, att, peak, total, acc, w_out, w_gate, w_up, w_down, x, hidden, mix,
                 send_half, got_half, kept, send_sum, got_sum,
                 kvz_s, kvz_r, qz_s, qz_r, kvx_s, kvx_r, loc, o_s, o_r,
                 wz_s, wz_r, wx_s, wx_r, own_w, wy_s, wy_r, wc_s, wc_r,
                 ag_s, ag_r, agc_s, agc_r, rc_s, rc_r, r2_s, r2_r):
    slots, group, m, n = plan.slots, plan.group, plan.m, plan.n
    tokens, rows, chips, depth = plan.tokens, plan.rows, plan.chips, plan.depth
    features = plan.features
    s = lax.axis_index("sp")
    t = lax.axis_index("tp")
    a, b = s // group, lax.rem(s, group)
    y, c = t // 2, lax.rem(t, 2)
    parity = lax.rem(a, 2)
    partner = y * 2 + 1 - c
    aside = lax.rem(s + 1, n)
    mine = pl.ds(pl.multiple_of(s * tokens, tokens), tokens)
    large = a < 0
    for i, k in enumerate(plan.keys):
        if k == 2:
            large = jnp.logical_or(large, a == i)
    by_kind = ((1, jnp.logical_not(large)), (2, large))
    by_parity = ((0, parity == 0), (1, parity == 1))

    def remote(src, dst, send, recv, sp, tp):
        return pltpu.make_async_remote_copy(
            src_ref=src, dst_ref=dst, send_sem=send, recv_sem=recv,
            device_id={"sp": sp, "tp": tp}, device_id_type=MESH)

    def arrival(dst, recv):
        remote(dst, dst, kvz_s.at[0], recv, aside, t).wait_recv()

    def block_of(i):
        return pl.ds(pl.multiple_of((i * group + b) * tokens, tokens), tokens)

    def kv_z(i):
        k = plan.keys[i]
        return remote(planes.at[pl.ds(plan.starts[i], k + 1)], kv.at[pl.ds(0, k + 1), mine],
                      kvz_s.at[i], kvz_r.at[a], i * group + b, t)

    def q_z(i):
        k = plan.keys[i]
        return remote(planes.at[pl.ds(plan.starts[i] + k + 1, k)], q.at[pl.ds(0, k), a],
                      qz_s.at[i], qz_r.at[a], i * group + b, t)

    def kv_own(i):
        k = plan.keys[i]
        return pltpu.make_async_copy(
            planes.at[pl.ds(plan.starts[i], k + 1)], kv.at[pl.ds(0, k + 1), mine], loc.at[0])

    def q_own(i):
        k = plan.keys[i]
        return pltpu.make_async_copy(
            planes.at[pl.ds(plan.starts[i] + k + 1, k)], q.at[pl.ds(0, k), a], loc.at[1])

    def peer(j):
        return a * group + lax.rem(b + j, group)

    def kv_x(k, i, j):
        part = kv.at[pl.ds(0, k + 1), block_of(i)]
        return remote(part, part, kvx_s.at[i, j - 1], kvx_r.at[i, j - 1], peer(j), t)

    pieces = 6

    def piece_in(k, par):
        tensor, h = k // 2, k % 2
        if tensor < 2:
            return (gate, up)[tensor].at[
                pl.ds(h * (depth // 2), depth // 2), pl.ds(plan.offsets[par], plan.sizes[par])]
        size = plan.sizes[par] // 2
        return down.at[pl.ds(plan.offsets[par] + h * size, size), :]

    def piece_at(k, par, block):
        tensor, h = k // 2, k % 2
        if tensor < 2:
            start = pl.multiple_of(block * depth + h * (depth // 2), depth // 2)
            return (w_gate, w_up)[tensor].at[pl.ds(start, depth // 2), pl.ds(0, plan.sizes[par])]
        size = plan.sizes[par] // 2
        return w_down.at[pl.ds(h * size, size), pl.ds(pl.multiple_of(block * depth, depth), depth)]

    def w_z(k, i):
        return remote(piece_in(k, i % 2), piece_at(k, i % 2, s), wz_s.at[k, i], wz_r.at[k, a],
                      i * group + b, t)

    def w_own(k, par):
        return pltpu.make_async_copy(piece_in(k, par), piece_at(k, par, s), own_w.at[k])

    def w_x(k, par, i, j):
        part = piece_at(k, par, i * group + b)
        return remote(part, part, wx_s.at[k, i, j - 1], wx_r.at[k, i, j - 1], peer(j), t)

    def w_start(k):
        for i in plan.order:
            @pl.when(a != i)
            def _():
                w_z(k, i).start()

    def w_forward(k):
        for par, when in by_parity:
            @pl.when(when)
            def _():
                for i in range(slots):
                    @pl.when(a == i)
                    def _():
                        w_own(k, par).wait()

                    @pl.when(a != i)
                    def _():
                        arrival(piece_at(k, par, i * group + b), wz_r.at[k, i])

                    for j in range(1, group):
                        w_x(k, par, i, j).start()

    def w_wait(k):
        for par, when in by_parity:
            @pl.when(when)
            def _():
                for i in range(slots):
                    for j in range(1, group):
                        block = i * group + lax.rem(b + group - j, group)
                        arrival(piece_at(k, par, block), wx_r.at[k, i, j - 1])

    def tp_of(dy):
        return lax.rem(y + dy, chips) * 2 + c

    def wo_y(dy):
        return remote(out_w, w_out.at[t], wy_s.at[dy - 1], wy_r.at[chips - dy - 1], s, tp_of(dy))

    def wo_c(dy):
        part = w_out.at[tp_of(dy)]
        return remote(out_w if dy == 0 else part, part, wc_s.at[dy], wc_r.at[dy], s, partner)

    def wo_own():
        return pltpu.make_async_copy(out_w, w_out.at[t], loc.at[2])

    def other(r):
        dz, dy = r // chips, r % chips
        slot = a + dz * (1 - 2 * parity)
        return slot * group + b, tp_of(dy)

    def back(r):
        dz, dy = r // chips, r % chips
        return dz * chips + (chips - dy) % chips

    def row_far(r):
        sp, tp = other(r)
        return remote(x.at[0, 0], x.at[back(r), 0], ag_s.at[r], ag_r.at[back(r)], sp, tp)

    def row_near(r):
        return remote(x.at[r, 0], x.at[r, 1], agc_s.at[r], agc_r.at[r], s, partner)

    def half_near(r):
        return remote(send_half.at[r], got_half.at[r], rc_s.at[r], rc_r.at[r], s, partner)

    def sum_far(r):
        sp, tp = other(r)
        return remote(send_sum.at[r], got_sum.at[back(r)], r2_s.at[r], r2_r.at[back(r)], sp, tp)

    for i in range(slots):
        @pl.when(a == i)
        def _():
            kv_own(i).start()
            q_own(i).start()
    for i in plan.order:
        @pl.when(a != i)
        def _():
            kv_z(i).start()
    for i in plan.order:
        @pl.when(a != i)
        def _():
            q_z(i).start()
    for dy in range(1, chips):
        wo_y(dy).start()
    wo_c(0).start()
    wo_own().start()
    for par, when in by_parity:
        @pl.when(when)
        def _():
            for k in range(pieces):
                w_own(k, par).start()
    if plan.sizes[1] < plan.sizes[0]:
        @pl.when(parity == 1)
        def _():
            spare = pl.ds(plan.sizes[1], plan.sizes[0] - plan.sizes[1])
            w_gate[:, spare] = jnp.zeros((features, plan.sizes[0] - plan.sizes[1]), w_gate.dtype)
            w_up[:, spare] = jnp.zeros((features, plan.sizes[0] - plan.sizes[1]), w_up.dtype)
            w_down[spare, :] = jnp.zeros((plan.sizes[0] - plan.sizes[1], features), w_down.dtype)

    for i in range(slots):
        @pl.when(a == i)
        def _():
            kv_own(i).wait()
            q_own(i).wait()
            for j in range(1, group):
                kv_x(plan.keys[i], i, j).start()

    w_start(0)

    for distance in range(1, slots):
        for i in range(slots):
            @pl.when(jnp.abs(a - i) == distance)
            def _():
                for k, when in by_kind:
                    @pl.when(when)
                    def _():
                        arrival(kv.at[pl.ds(0, k + 1), block_of(i)], kvz_r.at[i])
                        for j in range(1, group):
                            kv_x(k, i, j).start()
    w_start(1)

    for k, when in by_kind:
        @pl.when(when)
        def _():
            for i in range(slots):
                @pl.when(a != i)
                def _():
                    arrival(q.at[pl.ds(0, k), i], qz_r.at[i])

                for j in range(1, group):
                    block = i * group + lax.rem(b + group - j, group)
                    from_peer = pl.ds(pl.multiple_of(block * tokens, tokens), tokens)
                    arrival(kv.at[pl.ds(0, k + 1), from_peer], kvx_r.at[i, j - 1])

    @pl.when(jnp.logical_not(large))
    def _():
        for i in range(slots):
            both = q[0, i]
            lane = lax.broadcasted_iota(jnp.int32, both.shape, 1)
            q[1, i] = jnp.where(lane >= plan.small_size, both, jnp.zeros_like(both))
            q[0, i] = jnp.where(lane < plan.small_size, both, jnp.zeros_like(both))

    lift = large.astype(jnp.int32)
    factor = jnp.where(large, plan.large_size**-0.5 * log2_e, plan.small_size**-0.5 * log2_e)
    lam = lam_ref[a]
    last = (((1,), (1,)), ((), ()))
    high = min(256, tokens)
    parts = tokens // high
    owners = high // rows
    head = t * slots + a

    def o_copy(i, which):
        return remote(o.at[i, pl.ds(pl.multiple_of(which * rows, rows), rows)], att.at[head],
                      o_s.at[i, which], o_r.at[head], i * group + b, which)

    def attend(step):
        i, part = step // parts, lax.rem(step, parts)
        block = i * group + b
        row0 = part * high
        here = pl.ds(pl.multiple_of(row0, high), high)
        queries = (q[0, i, here], q[1, i, here])

        def score(which, start):
            keys = kv[which * lift, pl.ds(pl.multiple_of(start, tokens), tokens)]
            return lax.dot_general(queries[which], keys, last, preferred_element_type=jnp.float32)

        def masked(which):
            near = score(which, block * tokens)
            row = row0 + lax.broadcasted_iota(jnp.int32, near.shape, 0)
            column = lax.broadcasted_iota(jnp.int32, near.shape, 1)
            return jnp.where(column <= row, near, masked_score)

        for which in range(2):
            peak[which] = fold_lanes(masked(which), jnp.maximum)

        def find(chunk, carry):
            for which in range(2):
                peak[which] = jnp.maximum(
                    peak[which], fold_lanes(score(which, chunk * tokens), jnp.maximum))
            return carry

        lax.fori_loop(0, block, find, 0)
        tops = [jnp.max(peak[which], axis=1, keepdims=True) for which in range(2)]
        for which in range(2):
            peak[which] = jnp.broadcast_to(tops[which], (high, 128))

        def weigh(which, values, start, first):
            top = peak[which][:, :1]
            weights = jnp.exp2((values - top) * factor)
            value = kv[1 + lift, pl.ds(pl.multiple_of(start, tokens), tokens)]
            part_sum = fold_lanes(weights, jnp.add)
            part_acc = jnp.dot(weights.astype(jnp.bfloat16), value, preferred_element_type=jnp.float32)
            if first:
                total[which] = part_sum
                acc[which] = part_acc
            else:
                total[which] += part_sum
                acc[which] += part_acc

        for which in range(2):
            weigh(which, masked(which), block * tokens, True)

        def far(chunk, carry):
            for which in range(2):
                weigh(which, score(which, chunk * tokens), chunk * tokens, False)
            return carry

        lax.fori_loop(0, block, far, 0)
        outs = [acc[which] / jnp.sum(total[which], axis=1, keepdims=True) for which in range(2)]
        combined = outs[0] - lam * outs[1]
        mean_square = jnp.mean(combined * combined, axis=1, keepdims=True)
        normed = combined * lax.rsqrt(mean_square + norm_epsilon) * gain_ref[...] * branch_scale
        o[i, here] = normed.astype(o.dtype)

    def send(step):
        i, part = step // parts, lax.rem(step, parts)
        for w in range(owners):
            which = part * owners + w

            @pl.when(jnp.logical_not(jnp.logical_and(i == a, which == t)))
            def _():
                o_copy(i, which).start()

    steps = slots * parts
    plan_at = {}
    plan_at.setdefault(steps // 2, []).append(functools.partial(w_start, 2))
    plan_at.setdefault(steps * 5 // 8, []).append(functools.partial(w_forward, 0))
    plan_at.setdefault(steps * 7 // 8, []).append(functools.partial(w_forward, 1))

    def wo_forward():
        for dy in range(1, chips):
            arrival(w_out.at[tp_of(dy)], wy_r.at[dy - 1])
            wo_c(dy).start()

    plan_at.setdefault(steps * 6 // 8, []).append(wo_forward)

    def step_body(step, carry):
        for at, actions in plan_at.items():
            @pl.when(step == at)
            def _():
                for action in actions:
                    action()
        attend(step)

        @pl.when(step > 0)
        def _():
            send(step - 1)

        return carry

    lax.fori_loop(0, steps, step_body, 0)
    att[head] = o[a, pl.ds(pl.multiple_of(t * rows, rows), rows)]
    send(steps - 1)
    w_start(3)
    w_forward(2)

    wo_own().wait()
    for dy in range(chips):
        block = lax.rem(y + dy, chips) * 2 + 1 - c
        arrival(w_out.at[block], wc_r.at[dy])
    for h in range(m * slots):
        @pl.when(head != h)
        def _():
            arrival(att.at[h], o_r.at[h])
    wide = 512
    for start in range(0, features, wide):
        cols = pl.ds(start, wide)
        sums = None
        for tt in range(m):
            left = jnp.concatenate([att[tt * slots + i] for i in range(slots)], axis=1)
            term = jnp.dot(left, w_out[tt, :, cols], preferred_element_type=jnp.float32)
            sums = term if sums is None else sums + term
        mix[:, cols] = residual_scale * residual_ref[:, cols].astype(jnp.float32) + sums
    x[0, 0] = layer_norm(mix[...], norm_ref[...]).astype(x.dtype)
    for r in reversed(range(1, plan.peers)):
        row_far(r).start()
    row_near(0).start()
    w_start(4)
    w_start(5)
    w_forward(3)

    for k in range(4):
        w_wait(k)
    units = plan.sizes[0]
    span = 256 if units % 256 == 0 else 128

    def gate_up(r):
        both = x[r].reshape(2 * rows, features)
        for start in range(0, units, span):
            cols = pl.ds(start, span)
            g = jnp.dot(both, w_gate[:, cols], preferred_element_type=jnp.float32)
            u = jnp.dot(both, w_up[:, cols], preferred_element_type=jnp.float32)
            hidden[r, :, cols] = (g / (1.0 + jnp.exp(-g)) * u).astype(hidden.dtype)

    def gate_up_step(r, carry):
        @pl.when(r > 0)
        def _():
            arrival(x.at[r, 0], ag_r.at[r])
            row_near(r).start()

        arrival(x.at[r, 1], agc_r.at[r])
        gate_up(r)
        return carry

    lax.fori_loop(0, plan.peers, gate_up_step, 0)

    for k in (4, 5):
        w_forward(k)
    for k in (4, 5):
        w_wait(k)

    def down_rows(r):
        for start in range(0, features, wide):
            cols = pl.ds(start, wide)
            part = jnp.dot(hidden[r], w_down[:, cols], preferred_element_type=jnp.float32)
            kept[r, :, cols] = part[:rows]
            send_half[r, :, cols] = part[rows:].astype(send_half.dtype)

    def pass_on(r):
        arrival(got_half.at[r], rc_r.at[r])
        send_sum[r] = (kept[r] + got_half[r].astype(jnp.float32)).astype(send_sum.dtype)

    peers = plan.peers

    for back_r in range(peers):
        r = peers - 1 - back_r
        down_rows(r)
        half_near(r).start()
        if back_r > 0:
            pass_on(r + 1)
            sum_far(r + 1).start()
    arrival(got_half.at[0], rc_r.at[0])
    result = kept[0] + got_half[0].astype(jnp.float32)
    for r in range(1, peers):
        arrival(got_sum.at[r], r2_r.at[r])
        result += got_sum[r].astype(jnp.float32)
    out_ref[...] = (
        residual_scale * x[0, 0].astype(jnp.float32) + 0.5 * result).astype(out_ref.dtype)

    for i in range(slots):
        @pl.when(a != i)
        def _():
            kv_z(i).wait_send()
            q_z(i).wait_send()
            for k in range(pieces):
                w_z(k, i).wait_send()

        for k, when in by_kind:
            @pl.when(when)
            def _():
                for j in range(1, group):
                    kv_x(k, i, j).wait_send()
        for par, when in by_parity:
            @pl.when(when)
            def _():
                for j in range(1, group):
                    for k in range(pieces):
                        w_x(k, par, i, j).wait_send()
        for which in range(parts * owners):
            @pl.when(jnp.logical_not(jnp.logical_and(i == a, which == t)))
            def _():
                o_copy(i, which).wait_send()
    for dy in range(1, chips):
        wo_y(dy).wait_send()
    for dy in range(chips):
        wo_c(dy).wait_send()
    for r in range(peers):
        row_near(r).wait_send()
        half_near(r).wait_send()
        if r > 0:
            row_far(r).wait_send()
            sum_far(r).wait_send()


def run_layer(plan, lams, planes, gain, out_w, residual, norm_gain, gate, up, down, width):
    dma = pltpu.SemaphoreType.DMA
    slots, n, m, peers, chips = plan.slots, plan.n, plan.m, plan.peers, plan.chips
    rows, features, units = plan.rows, plan.features, plan.sizes[0]
    high = min(256, plan.tokens)
    anywhere = pl.BlockSpec(memory_space=pl.ANY)
    vmem = pl.BlockSpec(memory_space=pltpu.VMEM)
    others = max(plan.group - 1, 1)
    bf16, f32 = jnp.bfloat16, jnp.float32
    return pl.pallas_call(
        functools.partial(layer_kernel, plan),
        out_shape=jax.ShapeDtypeStruct((rows, features), bf16),
        in_specs=[pl.BlockSpec(memory_space=pltpu.SMEM), anywhere, vmem, anywhere, vmem, vmem,
                  anywhere, anywhere, anywhere],
        out_specs=vmem,
        scratch_shapes=[
            pltpu.VMEM((3, n * plan.tokens, width), bf16),
            pltpu.VMEM((2, slots, plan.tokens, width), bf16),
            pltpu.VMEM((slots, plan.tokens, width), bf16),
            pltpu.VMEM((m * slots, rows, width), bf16),
            pltpu.VMEM((2, high, 128), f32),
            pltpu.VMEM((2, high, 128), f32),
            pltpu.VMEM((2, high, width), f32),
            pltpu.VMEM((m, slots * width, features), bf16),
            pltpu.VMEM((features, units), bf16),
            pltpu.VMEM((features, units), bf16),
            pltpu.VMEM((units, features), bf16),
            pltpu.VMEM((peers, 2, rows, features), bf16),
            pltpu.VMEM((peers, 2 * rows, units), bf16),
            pltpu.VMEM((rows, features), f32),
            pltpu.VMEM((peers, rows, features), bf16),
            pltpu.VMEM((peers, rows, features), bf16),
            pltpu.VMEM((peers, rows, features), f32),
            pltpu.VMEM((peers, rows, features), bf16),
            pltpu.VMEM((peers, rows, features), bf16),
            dma((slots,)), dma((slots,)), dma((slots,)), dma((slots,)),
            dma((slots, others)), dma((slots, others)),
            dma((3,)),
            dma((slots, plan.tokens // rows)), dma((m * slots,)),
            dma((6, slots)), dma((6, slots)), dma((6, slots, others)), dma((6, slots, others)),
            dma((6,)),
            dma((max(chips - 1, 1),)), dma((max(chips - 1, 1),)), dma((chips,)), dma((chips,)),
            dma((peers,)), dma((peers,)), dma((peers,)), dma((peers,)),
            dma((peers,)), dma((peers,)), dma((peers,)), dma((peers,)),
        ],
        compiler_params=pltpu.CompilerParams(
            vmem_limit_bytes=60 * 2**20, has_side_effects=True),
        cost_estimate=pl.CostEstimate(
            flops=60_000_000_000, bytes_accessed=planes.size * 2, transcendentals=8_000_000),
        name="layer",
    )(lams, planes, gain.reshape(1, width), out_w, residual, norm_gain.reshape(1, features),
      gate, up, down)


def per_device(
    residual, query_small, key_small, value_small, query_large, key_large, value_large,
    lambda_small, lambda_large, head_gain, output_small, output_large, norm_gain,
    gate_weight, up_weight, down_weight,
):
    tokens, heads_small, width = value_small.shape
    heads_large = value_large.shape[1]
    rows, features = residual.shape
    n, m = lax.axis_size("sp"), lax.axis_size("tp")
    plan = Plan(n, m, heads_small, heads_large, tokens, rows,
                query_small.shape[2] // 2, query_large.shape[2] // 2)
    half = plan.large_size
    planes, lams, weights = [], [], []
    for kind, i in plan.kinds:
        if kind == "s":
            planes += [key_small[:, i], value_small[:, i], query_small[:, i]]
            lams.append(lambda_small[i])
            weights.append(output_small[i * width : (i + 1) * width])
        else:
            planes += [key_large[:, i, :half], key_large[:, i, half:], value_large[:, i],
                       query_large[:, i, :half], query_large[:, i, half:]]
            lams.append(lambda_large[i])
            weights.append(output_large[i * width : (i + 1) * width])
    short = -gate_weight.shape[1] % 128
    if short:
        gate_weight = jnp.pad(gate_weight, ((0, 0), (0, short)))
        up_weight = jnp.pad(up_weight, ((0, 0), (0, short)))
        down_weight = jnp.pad(down_weight, ((0, short), (0, 0)))
    plan.mixer(features, gate_weight.shape[1])
    return run_layer(
        plan, jnp.stack(lams), jnp.stack(planes), head_gain, jnp.concatenate(weights, axis=0),
        residual, norm_gain, gate_weight, up_weight, down_weight, width)


def solution(mesh):
    in_specs = (
        P(("sp", "tp"), None), P("sp", "tp", None), P("sp", "tp", None), P("sp", "tp", None),
        P("sp", "tp", None), P("sp", "tp", None), P("sp", "tp", None), P("tp"), P("tp"), P(),
        P("tp", None), P("tp", None), P(), P("sp", "tp"), P("sp", "tp"), P("tp", "sp"),
    )

    return jax.shard_map(
        per_device, mesh=mesh, in_specs=in_specs, out_specs=P(("sp", "tp"), None), check_vma=False
    )
```

time: 403 us -> 250 us (0.62)
  waiting for transfers between devices: 247 us -> 0 us
  Pallas kernels: 93.1 us -> 233 us
  matrix products: 27.2 us -> 0 us
  between operations: 13.5 us -> 0.24 us
  starting transfers between devices: 8.14 us -> 0 us
    all_gather x4 -> x0, waiting for transfers between devices: 215 us -> none  [the longest x1 92.6 us: per_device(): gate_full = lax.all_gather(gate_weight, 'sp', axis=0, tiled=True)]
    pallas_call x1, Pallas kernels: 93.1 us -> 233 us  [run_layer(): pl.pallas_call(functools.partial(layer_kernel, plan), out_shape=jax.Shape...]
    ppermute x4 -> x0, waiting for transfers between devices: 29.5 us -> none  [swap(): return lax.ppermute(value, axis, pairs)]
    dot_general x3 -> x0, matrix products: 27.2 us -> none  [the longest x1 14.8 us: per_device(): jnp.dot(hidden, down_full, preferred_element_type=jnp.float32)]
    ppermute x4 -> x0, starting transfers between devices: 8.02 us -> none  [swap(): return lax.ppermute(value, axis, pairs)]
  transfers between devices with their start and end apart: 8 -> 0, of which waited for: 7 -> 0; matrix products, arithmetic and copies ran while one was open for 5% -> 0% of each run, Pallas kernels for 23% -> 0%
where the time goes in v1:
time: 250 us; the launch traced here: 246 us
  Pallas kernels  233 us (93%)
  local copies, waits for them, and re-layouts  9.47 us (4%)
  other arithmetic  3.58 us (1%)
    pallas_call x1, Pallas kernels, run_layer(): pl.pallas_call(functools.partial(layer_kernel, plan), out_shape=jax.Shape...  233 us

profile of v1, /device:TPU:0, one launch (start us, length us, event | category | flops | bytes accessed | tf_op | source)
XLA Modules:
  0.0 246.2 jit_solution(4993250296816227518)
XLA Ops:
  0.0 0.0 copy-start.3
  0.0 0.0 copy-start
  0.0 1.6 fusion.21
  1.6 1.5 fusion.20
  3.1 0.0 copy-done.3
  3.1 0.0 copy-start.4
  3.1 0.4 fusion.19
  3.5 0.0 copy-done
  3.6 0.0 copy-start.1
  3.6 0.7 fusion.18
  4.4 0.0 copy-done.4
  4.4 0.4 fusion.22
  4.8 0.0 copy-done.1
  4.8 0.7 fusion.17
  5.6 0.0 copy-start.2
  5.7 0.0 copy-start.5
  5.9 0.8 copy-done.2
  6.8 0.0 copy-start.6
  6.8 0.1 fusion.16
  6.9 0.3 copy-done.5
  7.1 0.0 copy-start.7
  7.1 0.0 copy-start.8
  7.2 1.6 pad_maximum_fusion.out_w
  8.7 0.0 copy-done.6
  8.8 0.0 copy-done.7
  8.8 0.7 fusion.23
  9.4 0.0 copy-done.8
  9.4 2.0 pad_maximum_fusion.1.lam_ref
  11.4 232.9 %layer.1 = bf16[128,2048]{1,0:T(8,128)(2,1)} custom-call(f32[4]{0:T(128)} %pad_maximum_fusion.1.lam_ref, bf16[16,512,128]{2,1,0:T(8,128)(2,1)} %copy-done.6, f32[1,128]{1,0:T(1,128)} %bitcast.67, bf16[512,2048]{1,0:T(8,128)(2,1)} %pad_maximum_fusion.out_w, bf16[128,2048]{1,0:T(8,128)(2,1)} %residual_ref.1, f32[1,2048]{1,0:T(1,128)} %bitcast.66, ...), custom_call_target="tpu_custom_call" | custom-call | flops 60000002048 | bytes 2097152 | tf_op jit(solution)/shard_map/layer/pallas_call | solution.py:539
  244.3 1.9 copy.113
  (16 shorter events, 0.5 us)
Async XLA Ops:
  0.0 3.1 %copy-start.3 = (bf16[512,2,128]{2,1,0:T(2,128)(2,1)S(1)}, bf16[512,2,128]{2,1,0:T(2,128)(2,1)}, u32[]{:S(2)}) copy-start(bf16[512,2,128]{2,1,0:T(2,128)(2,1)} %param.17) | copy-start | bytes 786436
  0.0 3.5 %copy-start = (bf16[512,2,256]{2,1,0:T(2,128)(2,1)S(1)}, bf16[512,2,256]{2,1,0:T(2,128)(2,1)}, u32[]{:S(2)}) copy-start(bf16[512,2,256]{2,1,0:T(2,128)(2,1)} %param.21) | copy-start | bytes 1572868
  3.1 1.3 copy-start.4
  3.6 1.2 copy-start.1
  5.6 1.2 copy-start.2
  5.7 1.4 copy-start.5
  6.8 2.0 copy-start.6
  7.1 1.6 copy-start.7
  7.1 2.3 copy-start.8

commit v2 on v1

v2 whole, which is shorter than its diff:
```python
import functools

import jax
import jax.numpy as jnp
from jax import lax
from jax.experimental import pallas as pl
from jax.experimental.pallas import tpu as pltpu
from jax.sharding import PartitionSpec as P

residual_scale = 8.0**0.25
branch_scale = 0.8
norm_epsilon = 1e-05
masked_score = -1e30
log2_e = 1.4426950408889634
MESH = pl.DeviceIdType.MESH


def layer_norm(values, gains):
    centered = values - jnp.mean(values, axis=-1, keepdims=True)
    variance = jnp.mean(centered * centered, axis=-1, keepdims=True)
    return centered * lax.rsqrt(variance + norm_epsilon) * gains


def fold_lanes(values, op):
    result = values[:, :128]
    for start in range(128, values.shape[1], 128):
        result = op(result, values[:, start : start + 128])
    return result


class Plan:
    def __init__(self, n, m, small, large, tokens, rows, small_size, large_size, features, units):
        self.n, self.m, self.chips, self.peers = n, m, m // 2, m
        self.slots = small + large
        self.group = n // self.slots
        half = small // 2
        self.kinds = [("s", i) for i in range(half)]
        self.kinds += [("l", i) for i in range(large)]
        self.kinds += [("s", i) for i in range(half, small)]
        self.keys = [1 if kind == "s" else 2 for kind, _ in self.kinds]
        self.natural = [self.kinds.index(("s", i)) for i in range(small)]
        self.natural += [self.kinds.index(("l", i)) for i in range(large)]
        self.tokens, self.rows, self.features = tokens, rows, features
        self.small_size, self.large_size = small_size, large_size
        tiles = units // 128
        first = (tiles + 1) // 2 * 128
        self.sizes, self.offsets = (first, units - first), (0, first)
        self.depth = features // n
        self.halves = max(1, self.depth // 128)
        self.span = self.depth // self.halves
        self.columns = [(start, tuple(max(0, min(256, size - start)) for size in self.sizes))
                        for start in range(0, first, 256)]
        self.pieces = [(tensor, j) for j in range(len(self.columns)) for tensor in (0, 1)]
        self.ups = len(self.pieces)
        self.pieces += [(2, (h, part)) for h in range(self.halves) for part in range(2)]
        keys = n * tokens
        self.high = tokens
        while self.high > 128 and self.high * keys > 2**21:
            self.high //= 2


def layer_kernel(plan, lam_small, lam_large, k_small, v_small, q_small, k_large, v_large, q_large, gain_ref,
                 out_small, out_large, residual_ref, norm_ref, gate, up, down, out_ref,
                 kv, q, o, att, pool, peak, total, acc, w_out, w_gate, w_up, w_down, x, hidden,
                 send_half, got_half, send_sum, got_sum,
                 kz_s, kz_r, vz_s, vz_r, qz_s, qz_r, kx_s, kx_r, vx_s, vx_r, loc, o_s, o_r,
                 wz_s, wz_r, wx_s, wx_r, own_w, wy_s, wy_r, wc_s, wc_r,
                 ag_s, ag_r, agc_s, agc_r, rc_s, rc_r, r2_s, r2_r):
    slots, group, m, n = plan.slots, plan.group, plan.m, plan.n
    tokens, rows, chips, depth = plan.tokens, plan.rows, plan.chips, plan.depth
    features = plan.features
    s = lax.axis_index("sp")
    t = lax.axis_index("tp")
    a, b = s // group, lax.rem(s, group)
    y, c = t // 2, lax.rem(t, 2)
    parity = lax.rem(a, 2)
    partner = y * 2 + 1 - c
    aside = lax.rem(s + 1, n)
    mine = pl.ds(pl.multiple_of(s * tokens, tokens), tokens)
    large = a < 0
    for i, k in enumerate(plan.keys):
        if k == 2:
            large = jnp.logical_or(large, a == i)
    by_kind = ((1, jnp.logical_not(large)), (2, large))
    by_parity = ((0, parity == 0), (1, parity == 1))

    def remote(src, dst, send, recv, sp, tp):
        return pltpu.make_async_remote_copy(
            src_ref=src, dst_ref=dst, send_sem=send, recv_sem=recv,
            device_id={"sp": sp, "tp": tp}, device_id_type=MESH)

    def arrival(dst, recv):
        remote(dst, dst, kz_s.at[0], recv, aside, t).wait_recv()

    def block_of(i):
        return pl.ds(pl.multiple_of((i * group + b) * tokens, tokens), tokens)

    def source(i, what):
        kind, index = plan.kinds[i]
        return {"s": (k_small, v_small, q_small), "l": (k_large, v_large, q_large)}[kind][what].at[index]

    def to_slot(i, what):
        keys = pl.ds(0, plan.keys[i])
        dst = (kv.at[keys, mine], kv.at[pl.ds(2, 1), mine], q.at[keys, a])[what]
        send, recv = ((kz_s, kz_r), (vz_s, vz_r), (qz_s, qz_r))[what]
        return remote(source(i, what), dst, send.at[i], recv.at[a], i * group + b, t)

    def to_self(i, what):
        keys = pl.ds(0, plan.keys[i])
        dst = (kv.at[keys, mine], kv.at[pl.ds(2, 1), mine], q.at[keys, a])[what]
        return pltpu.make_async_copy(source(i, what), dst, loc.at[what])

    def peer(j):
        return a * group + lax.rem(b + j, group)

    def k_x(k, i, j):
        part = kv.at[pl.ds(0, k), block_of(i)]
        return remote(part, part, kx_s.at[i, j - 1], kx_r.at[i, j - 1], peer(j), t)

    def v_x(i, j):
        part = kv.at[pl.ds(2, 1), block_of(i)]
        return remote(part, part, vx_s.at[i, j - 1], vx_r.at[i, j - 1], peer(j), t)

    pieces = len(plan.pieces)

    def piece_in(k, par):
        tensor, which = plan.pieces[k]
        if tensor < 2:
            start, widths = plan.columns[which]
            return (gate, up)[tensor].at[:, pl.ds(plan.offsets[par] + start, widths[par])]
        h, part = which
        size = plan.sizes[par] // 2
        return down.at[pl.ds(plan.offsets[par] + part * size, size), pl.ds(h * plan.span, plan.span)]

    def piece_at(k, par, block):
        tensor, which = plan.pieces[k]
        if tensor < 2:
            start, widths = plan.columns[which]
            return (w_gate, w_up)[tensor].at[
                pl.ds(pl.multiple_of(block * depth, depth), depth), pl.ds(start, widths[par])]
        h, part = which
        size = plan.sizes[par] // 2
        return w_down.at[h, pl.ds(part * size, size),
                         pl.ds(pl.multiple_of(block * plan.span, plan.span), plan.span)]

    def w_z(k, i):
        return remote(piece_in(k, i % 2), piece_at(k, i % 2, s), wz_s.at[k, i], wz_r.at[k, a],
                      i * group + b, t)

    def w_own(k, par):
        return pltpu.make_async_copy(piece_in(k, par), piece_at(k, par, s), own_w.at[k])

    def w_x(k, par, i, j):
        part = piece_at(k, par, i * group + b)
        return remote(part, part, wx_s.at[k, i, j - 1], wx_r.at[k, i, j - 1], peer(j), t)

    def w_start(k):
        for distance in range(1, slots):
            for i in range(slots):
                @pl.when(jnp.abs(a - i) == distance)
                def _():
                    w_z(k, i).start()

    def w_share(k):
        for par, when in by_parity:
            @pl.when(when)
            def _():
                w_own(k, par).wait()
                for i in range(slots):
                    @pl.when(a == i)
                    def _():
                        for j in range(1, group):
                            w_x(k, par, i, j).start()

    def w_forward(k):
        for par, when in by_parity:
            @pl.when(when)
            def _():
                for distance in range(1, slots):
                    for i in range(slots):
                        @pl.when(jnp.abs(a - i) == distance)
                        def _():
                            arrival(piece_at(k, par, i * group + b), wz_r.at[k, i])
                            for j in range(1, group):
                                w_x(k, par, i, j).start()

    def w_wait(k):
        for par, when in by_parity:
            @pl.when(when)
            def _():
                for i in range(slots):
                    for j in range(1, group):
                        block = i * group + lax.rem(b + group - j, group)
                        arrival(piece_at(k, par, block), wx_r.at[k, i, j - 1])

    def tp_of(dy):
        return lax.rem(y + dy, chips) * 2 + c

    cut = out_small.shape[0]
    spans = ((out_small, pl.ds(0, cut)), (out_large, pl.ds(cut, out_large.shape[0])))

    def wo_y(dy, e):
        part, place = spans[e]
        return remote(part, w_out.at[t, place], wy_s.at[dy - 1, e], wy_r.at[chips - dy - 1, e], s, tp_of(dy))

    def wo_c(dy, e):
        part, place = spans[e]
        there = w_out.at[tp_of(dy), place]
        return remote(part if dy == 0 else there, there, wc_s.at[dy, e], wc_r.at[dy, e], s, partner)

    def wo_own(e):
        part, place = spans[e]
        return pltpu.make_async_copy(part, w_out.at[t, place], loc.at[3 + e])

    pair = (a + 1 - 2 * parity) * group + b

    def row_z():
        return remote(x.at[0, 0], x.at[chips, 0], ag_s.at[0], ag_r.at[chips], pair, t)

    def row_y(dz, dy):
        r = dz * chips + dy
        into = dz * chips + chips - dy
        return remote(x.at[dz * chips, 0], x.at[into, 0], ag_s.at[r], ag_r.at[into], s, tp_of(dy))

    def row_near(r):
        return remote(x.at[r, 0], x.at[r, 1], agc_s.at[r], agc_r.at[r], s, partner)

    def half_near(h, r):
        return remote(send_half.at[h, r], got_half.at[h, r], rc_s.at[h, r], rc_r.at[h, r], s, partner)

    def sum_y(h, dz, dy):
        into = dz * chips + chips - dy
        r = dz * chips + dy
        return remote(send_sum.at[h, r], got_sum.at[h, into], r2_s.at[h, r], r2_r.at[h, into], s, tp_of(dy))

    def sum_z(h):
        return remote(send_sum.at[h, chips], got_sum.at[h, 0], r2_s.at[h, 0], r2_r.at[h, 0], pair, t)

    barrier = pltpu.get_barrier_semaphore()
    for i in range(slots):
        for tt in range(m):
            @pl.when(jnp.logical_not(jnp.logical_and(i == a, tt == t)))
            def _():
                pl.semaphore_signal(barrier, inc=1, device_id={"sp": i * group + b, "tp": tt},
                                    device_id_type=MESH)
    for j in range(1, group):
        pl.semaphore_signal(barrier, inc=1, device_id={"sp": peer(j), "tp": t}, device_id_type=MESH)
    for i in range(slots):
        @pl.when(a == i)
        def _():
            for what in range(3):
                to_self(i, what).start()
    for e in range(2):
        wo_own(e).start()
    for par, when in by_parity:
        @pl.when(when)
        def _():
            for k in range(pieces):
                w_own(k, par).start()
    pl.semaphore_wait(barrier, slots * m - 1 + group - 1)

    for what in range(3):
        for distance in range(1, slots):
            for i in range(slots):
                @pl.when(jnp.abs(a - i) == distance)
                def _():
                    to_slot(i, what).start()
    w_start(0)
    for e in range(2):
        for dy in range(1, chips):
            wo_y(dy, e).start()
        wo_c(0, e).start()
    if plan.sizes[1] < plan.sizes[0]:
        @pl.when(parity == 1)
        def _():
            spare = pl.ds(plan.sizes[1], plan.sizes[0] - plan.sizes[1])
            w_gate[:, spare] = jnp.zeros((features, plan.sizes[0] - plan.sizes[1]), w_gate.dtype)
            w_up[:, spare] = jnp.zeros((features, plan.sizes[0] - plan.sizes[1]), w_up.dtype)
            for h in range(plan.halves):
                w_down[h, spare, :] = jnp.zeros(
                    (plan.sizes[0] - plan.sizes[1], features // plan.halves), w_down.dtype)

    for i in range(slots):
        @pl.when(a == i)
        def _():
            for what in range(3):
                to_self(i, what).wait()
            for j in range(1, group):
                k_x(plan.keys[i], i, j).start()
                v_x(i, j).start()

    for distance in range(1, slots):
        for i in range(slots):
            for k, when in by_kind:
                @pl.when(jnp.logical_and(when, jnp.abs(a - i) == distance))
                def _():
                    arrival(kv.at[pl.ds(0, k), block_of(i)], kz_r.at[i])
                    for j in range(1, group):
                        k_x(k, i, j).start()
    for distance in range(1, slots):
        for i in range(slots):
            @pl.when(jnp.abs(a - i) == distance)
            def _():
                arrival(kv.at[pl.ds(2, 1), block_of(i)], vz_r.at[i])
                for j in range(1, group):
                    v_x(i, j).start()

    w_start(1)
    w_start(2)
    for k in range(pieces):
        w_share(k)

    def ready(i):
        for k, when in by_kind:
            @pl.when(when)
            def _():
                @pl.when(a != i)
                def _():
                    arrival(q.at[pl.ds(0, k), i], qz_r.at[i])

                for j in range(1, group):
                    block = i * group + lax.rem(b + group - j, group)
                    from_peer = pl.ds(pl.multiple_of(block * tokens, tokens), tokens)
                    arrival(kv.at[pl.ds(0, k), from_peer], kx_r.at[i, j - 1])
                    arrival(kv.at[pl.ds(2, 1), from_peer], vx_r.at[i, j - 1])

        @pl.when(jnp.logical_not(large))
        def _():
            both = q[0, i]
            lane = lax.broadcasted_iota(jnp.int32, both.shape, 1)
            q[1, i] = jnp.where(lane >= plan.small_size, both, jnp.zeros_like(both))
            q[0, i] = jnp.where(lane < plan.small_size, both, jnp.zeros_like(both))

    lift = large.astype(jnp.int32)
    factor = jnp.where(large, plan.large_size**-0.5 * log2_e, plan.small_size**-0.5 * log2_e)
    lam = jnp.float32(0.0)
    for i, (kind, index) in enumerate(plan.kinds):
        lam = jnp.where(a == i, (lam_small if kind == "s" else lam_large)[index], lam)
    last = (((1,), (1,)), ((), ()))
    high = plan.high
    parts = tokens // high
    wide = group * tokens
    strip = min(512, tokens)
    head = t * slots + a

    def o_copy(i, which):
        return remote(o.at[i, pl.ds(pl.multiple_of(which * rows, rows), rows)], att.at[head],
                      o_s.at[i, which], o_r.at[head], i * group + b, which)

    def attend(i, part):
        row0 = part * high
        here = pl.ds(pl.multiple_of(row0, high), high)
        queries = (q[0, i, here], q[1, i, here])

        def find(chunk, last_one):
            for which in range(2):
                for off in range(0, wide, strip):
                    at = pl.ds(pl.multiple_of(chunk * wide + off, strip), strip)
                    score = lax.dot_general(
                        queries[which], kv[which * lift, at], last, preferred_element_type=jnp.float32)
                    if last_one:
                        row = b * tokens + row0 + lax.broadcasted_iota(jnp.int32, score.shape, 0)
                        column = off + lax.broadcasted_iota(jnp.int32, score.shape, 1)
                        score = jnp.where(column <= row, score, masked_score)
                    pool[which, :, at] = score
                    top = fold_lanes(score, jnp.maximum)
                    fresh = last_one and off == 0
                    peak[which] = top if fresh else jnp.maximum(peak[which], top)

        find(i, True)
        lax.fori_loop(0, i, lambda chunk, carry: find(chunk, False) or carry, 0)
        for which in range(2):
            peak[which] = jnp.broadcast_to(
                jnp.max(peak[which], axis=1, keepdims=True), (high, 128))

        def weigh(chunk, fresh):
            for which in range(2):
                sums = outs = None
                for off in range(0, wide, strip):
                    at = pl.ds(pl.multiple_of(chunk * wide + off, strip), strip)
                    score = pool[which, :, at]
                    top = peak[which]
                    weights = jnp.concatenate(
                        [jnp.exp2((score[:, u : u + 128] - top) * factor) for u in range(0, strip, 128)],
                        axis=1)
                    part_sum = fold_lanes(weights, jnp.add)
                    part_out = jnp.dot(
                        weights.astype(jnp.bfloat16), kv[2, at], preferred_element_type=jnp.float32)
                    sums = part_sum if sums is None else sums + part_sum
                    outs = part_out if outs is None else outs + part_out
                if fresh:
                    total[which], acc[which] = sums, outs
                else:
                    total[which] += sums
                    acc[which] += outs

        weigh(i, True)
        lax.fori_loop(0, i, lambda chunk, carry: weigh(chunk, False) or carry, 0)
        outs = [acc[which] / jnp.sum(total[which], axis=1, keepdims=True) for which in range(2)]
        combined = outs[0] - lam * outs[1]
        mean_square = jnp.mean(combined * combined, axis=1, keepdims=True)
        normed = combined * lax.rsqrt(mean_square + norm_epsilon) * gain_ref[...] * branch_scale
        o[i, here] = normed.astype(o.dtype)

    def send(i):
        for which in range(tokens // rows):
            @pl.when(jnp.logical_not(jnp.logical_and(i == a, which == t)))
            def _():
                o_copy(i, which).start()

    def wo_forward():
        for dy in range(1, chips):
            for e in range(2):
                place = spans[e][1]
                arrival(w_out.at[tp_of(dy), place], wy_r.at[dy - 1, e])
                wo_c(dy, e).start()

    def step_body(i, carry):
        for at in range(slots):
            @pl.when(i == at)
            def _():
                ready(at)
        lax.fori_loop(0, parts, lambda part, c: attend(i, part) or c, 0)

        @pl.when(i > 0)
        def _():
            send(i - 1)

        return carry

    lax.fori_loop(0, slots, step_body, 0)
    att[head] = o[a, pl.ds(pl.multiple_of(t * rows, rows), rows)]
    send(slots - 1)
    w_start(3)
    w_start(4)
    w_forward(0)
    wo_forward()
    w_forward(1)

    for e in range(2):
        wo_own(e).wait()
        for dy in range(chips):
            block = lax.rem(y + dy, chips) * 2 + 1 - c
            arrival(w_out.at[block, spans[e][1]], wc_r.at[dy, e])
    for h in range(m * slots):
        @pl.when(head != h)
        def _():
            arrival(att.at[h], o_r.at[h])
    stretch = 512
    base = plan.features
    for start in range(0, features, stretch):
        cols = pl.ds(start, stretch)
        sums = None
        for tt in range(m):
            left = jnp.concatenate([att[tt * slots + i] for i in plan.natural], axis=1)
            term = jnp.dot(left, w_out[tt, :, cols], preferred_element_type=jnp.float32)
            sums = term if sums is None else sums + term
        pool[1, pl.ds(0, rows), pl.ds(base + start, stretch)] = (
            residual_scale * residual_ref[:, cols].astype(jnp.float32) + sums)
    x[0, 0] = layer_norm(pool[1, pl.ds(0, rows), pl.ds(base, features)], norm_ref[...]).astype(x.dtype)
    peers = plan.peers
    row_z().start()
    for dy in range(1, chips):
        row_y(0, dy).start()
    row_near(0).start()
    for k in range(5, pieces):
        w_start(k)
    for k in range(2, plan.ups):
        w_forward(k)
    arrival(x.at[chips, 0], ag_r.at[chips])
    for dy in range(1, chips):
        row_y(1, dy).start()
    row_near(chips).start()
    w_forward(plan.ups)
    for dz in range(2):
        for dy in range(1, chips):
            r = dz * chips + dy
            arrival(x.at[r, 0], ag_r.at[r])
            row_near(r).start()
    w_forward(plan.ups + 1)
    for r in range(peers):
        arrival(x.at[r, 1], agc_r.at[r])

    def gate_up(j):
        start, widths = plan.columns[j]
        cols = pl.ds(start, max(widths))

        def one(r, carry):
            both = x[r].reshape(2 * rows, features)
            g = jnp.dot(both, w_gate[:, cols], preferred_element_type=jnp.float32)
            u = jnp.dot(both, w_up[:, cols], preferred_element_type=jnp.float32)
            hidden[r, :, cols] = (g / (1.0 + jnp.exp(-g)) * u).astype(hidden.dtype)
            return carry

        lax.fori_loop(0, peers, one, 0)

    done = plan.ups + 2
    for j in range(len(plan.columns)):
        w_wait(2 * j)
        w_wait(2 * j + 1)
        gate_up(j)
        if done < pieces and j + 1 < len(plan.columns):
            w_forward(done)
            done += 1

    low = features // plan.halves
    band = min(512, low)
    per_plane = high // rows

    def kept(r, cols):
        return pool.at[r // per_plane, pl.ds(r % per_plane * rows, rows), cols]

    def down_rows(h, r):
        for start in range(0, low, band):
            cols = pl.ds(start, band)
            part = jnp.dot(hidden[r], w_down[h, :, cols], preferred_element_type=jnp.float32)
            kept(r, pl.ds(h * low + start, band))[...] = part[:rows]
            send_half[h, r, :, cols] = part[rows:].astype(send_half.dtype)

    def near_sum(h, r):
        arrival(got_half.at[h, r], rc_r.at[h, r])
        return kept(r, pl.ds(h * low, low))[...] + got_half[h, r].astype(jnp.float32)

    def down_half(h):
        order = [dz * chips + dy for dz in (1, 0) for dy in list(range(1, chips)) + [0]]
        for r in order:
            down_rows(h, r)
            half_near(h, r).start()
        for r in order:
            if r % chips:
                send_sum[h, r] = near_sum(h, r).astype(send_sum.dtype)
                sum_y(h, r // chips, r % chips).start()

    def plane_sum(h, dz):
        result = near_sum(h, dz * chips)
        for dy in range(1, chips):
            r = dz * chips + dy
            arrival(got_sum.at[h, r], r2_r.at[h, r])
            result += got_sum[h, r].astype(jnp.float32)
        return result

    def pass_pair(h):
        send_sum[h, chips] = plane_sum(h, 1).astype(send_sum.dtype)
        sum_z(h).start()

    def finish(h):
        result = plane_sum(h, 0)
        arrival(got_sum.at[h, 0], r2_r.at[h, 0])
        result += got_sum[h, 0].astype(jnp.float32)
        for block in range(n):
            cols = pl.ds(block * depth + h * plan.span, plan.span)
            out_ref[:, cols] = (
                residual_scale * x[0, 0, :, cols].astype(jnp.float32)
                + 0.5 * result[:, block * plan.span : (block + 1) * plan.span]
            ).astype(out_ref.dtype)

    for h in range(plan.halves):
        first = plan.ups + 2 * h
        for k in range(done, first + 2):
            w_forward(k)
        done = max(done, first + 2)
        w_wait(first)
        w_wait(first + 1)
        if h > 0:
            pass_pair(h - 1)
        down_half(h)
    pass_pair(plan.halves - 1)
    for h in range(plan.halves):
        finish(h)

    for i in range(slots):
        @pl.when(a != i)
        def _():
            for what in range(3):
                to_slot(i, what).wait_send()
            for k in range(pieces):
                w_z(k, i).wait_send()

        for k, when in by_kind:
            @pl.when(when)
            def _():
                for j in range(1, group):
                    k_x(k, i, j).wait_send()
                    v_x(i, j).wait_send()
        for par, when in by_parity:
            @pl.when(when)
            def _():
                for j in range(1, group):
                    for k in range(pieces):
                        w_x(k, par, i, j).wait_send()
        for which in range(tokens // rows):
            @pl.when(jnp.logical_not(jnp.logical_and(i == a, which == t)))
            def _():
                o_copy(i, which).wait_send()
    for e in range(2):
        for dy in range(1, chips):
            wo_y(dy, e).wait_send()
        for dy in range(chips):
            wo_c(dy, e).wait_send()
    row_z().wait_send()
    for r in range(peers):
        row_near(r).wait_send()
        for h in range(plan.halves):
            half_near(h, r).wait_send()
        if r % chips:
            row_y(r // chips, r % chips).wait_send()
            for h in range(plan.halves):
                sum_y(h, r // chips, r % chips).wait_send()
    for h in range(plan.halves):
        sum_z(h).wait_send()


def run_layer(plan, lams, small, large, gain, outs, residual, norm_gain, mixer, width):
    dma = pltpu.SemaphoreType.DMA
    slots, n, m, peers, chips = plan.slots, plan.n, plan.m, plan.peers, plan.chips
    rows, features, units, halves = plan.rows, plan.features, plan.sizes[0], plan.halves
    high, pieces = plan.high, len(plan.pieces)
    anywhere = pl.BlockSpec(memory_space=pl.ANY)
    vmem = pl.BlockSpec(memory_space=pltpu.VMEM)
    smem = pl.BlockSpec(memory_space=pltpu.SMEM)
    others, ahead = max(plan.group - 1, 1), max(chips - 1, 1)
    bf16, f32 = jnp.bfloat16, jnp.float32
    return pl.pallas_call(
        functools.partial(layer_kernel, plan),
        out_shape=jax.ShapeDtypeStruct((rows, features), bf16),
        in_specs=[smem] * 2 + [anywhere] * 6 + [vmem] + [anywhere] * 2 + [vmem] * 2 + [anywhere] * 3,
        out_specs=vmem,
        scratch_shapes=[
            pltpu.VMEM((3, n * plan.tokens, width), bf16),
            pltpu.VMEM((2, slots, plan.tokens, width), bf16),
            pltpu.VMEM((slots, plan.tokens, width), bf16),
            pltpu.VMEM((m * slots, rows, width), bf16),
            pltpu.VMEM((2, high, n * plan.tokens), f32),
            pltpu.VMEM((2, high, 128), f32),
            pltpu.VMEM((2, high, 128), f32),
            pltpu.VMEM((2, high, width), f32),
            pltpu.VMEM((m, slots * width, features), bf16),
            pltpu.VMEM((features, units), bf16),
            pltpu.VMEM((features, units), bf16),
            pltpu.VMEM((halves, units, features // halves), bf16),
            pltpu.VMEM((peers, 2, rows, features), bf16),
            pltpu.VMEM((peers, 2 * rows, units), bf16),
        ] + [pltpu.VMEM((halves, peers, rows, features // halves), bf16)] * 4 + [
            dma((slots,)), dma((slots,)), dma((slots,)), dma((slots,)), dma((slots,)), dma((slots,)),
            dma((slots, others)), dma((slots, others)), dma((slots, others)), dma((slots, others)),
            dma((5,)),
            dma((slots, plan.tokens // rows)), dma((m * slots,)),
            dma((pieces, slots)), dma((pieces, slots)),
            dma((pieces, slots, others)), dma((pieces, slots, others)),
            dma((pieces,)),
            dma((ahead, 2)), dma((ahead, 2)), dma((chips, 2)), dma((chips, 2)),
            dma((peers,)), dma((peers,)), dma((peers,)), dma((peers,)),
            dma((halves, peers)), dma((halves, peers)), dma((halves, peers)), dma((halves, peers)),
        ],
        compiler_params=pltpu.CompilerParams(
            vmem_limit_bytes=61 * 2**20, has_side_effects=True, collective_id=0),
        cost_estimate=pl.CostEstimate(
            flops=60_000_000_000, bytes_accessed=16_000_000, transcendentals=8_000_000),
        name="layer",
    )(*lams, *small, *large, gain.reshape(1, width), *outs, residual, norm_gain.reshape(1, features), *mixer)


def per_device(
    residual, query_small, key_small, value_small, query_large, key_large, value_large,
    lambda_small, lambda_large, head_gain, output_small, output_large, norm_gain,
    gate_weight, up_weight, down_weight,
):
    tokens, heads_small, width = value_small.shape
    heads_large = value_large.shape[1]
    rows, features = residual.shape
    n, m = lax.axis_size("sp"), lax.axis_size("tp")
    short = -gate_weight.shape[1] % 128
    if short:
        gate_weight = jnp.pad(gate_weight, ((0, 0), (0, short)))
        up_weight = jnp.pad(up_weight, ((0, 0), (0, short)))
        down_weight = jnp.pad(down_weight, ((0, short), (0, 0)))
    plan = Plan(n, m, heads_small, heads_large, tokens, rows, query_small.shape[2] // 2,
                query_large.shape[2] // 2, features, gate_weight.shape[1])

    def by_head(values):
        parts = values.reshape(tokens, values.shape[1], -1, width)
        return jnp.transpose(parts, (1, 2, 0, 3))

    small = [by_head(v) for v in (key_small, value_small, query_small)]
    large = [by_head(v) for v in (key_large, value_large, query_large)]
    return run_layer(
        plan, (lambda_small, lambda_large), small, large, head_gain, (output_small, output_large),
        residual, norm_gain, (gate_weight, up_weight, down_weight), width)


def solution(mesh):
    in_specs = (
        P(("sp", "tp"), None), P("sp", "tp", None), P("sp", "tp", None), P("sp", "tp", None),
        P("sp", "tp", None), P("sp", "tp", None), P("sp", "tp", None), P("tp"), P("tp"), P(),
        P("tp", None), P("tp", None), P(), P("sp", "tp"), P("sp", "tp"), P("tp", "sp"),
    )

    return jax.shard_map(per_device, mesh=mesh, in_specs=in_specs, out_specs=P(("sp", "tp"), None), check_vma=False)
```

time: 250 us -> 211 us (0.84); the launches traced: 246 us -> 211 us
  Pallas kernels: 233 us -> 203 us
  other arithmetic: 3.58 us -> 0 us
    pallas_call x1, Pallas kernels: 233 us -> 203 us  [run_layer(): pl.pallas_call(functools.partial(layer_kernel, plan), out_shape=jax.Shape...]
    slice x8 -> x0, local copies, waits for them, and re-layouts: 6 us -> none  [the longest x3 3.4 us: per_device(): planes += [key_small[:, i], value_small[:, i], query_small[:, i]]]
where the time goes in v2:
time: 211 us
  Pallas kernels  203 us (96%)
  local copies, waits for them, and re-layouts  8.04 us (4%)
    pallas_call x1, Pallas kernels, run_layer(): pl.pallas_call(functools.partial(layer_kernel, plan), out_shape=jax.Shape...  203 us
    unnamed x13, local copies, waits for them, and re-layouts  4.3 us

profile of v2, /device:TPU:0, one launch (start us, length us, event | category | flops | bytes accessed | tf_op | source)
XLA Modules:
  0.0 210.6 jit_solution(6192923836893801317)
XLA Ops:
  0.0 1.3 copy.27
  1.3 0.0 copy-start
  1.3 1.0 copy.28
  2.3 0.0 copy-done
  2.4 0.7 copy.24
  3.1 0.0 copy-start.1
  3.1 0.0 copy-start.2
  3.1 1.0 copy.25
  4.1 0.0 copy-done.1
  4.1 0.0 copy-done.2
  4.1 0.0 copy-start.3
  4.1 0.0 copy-start.4
  4.1 0.9 copy_bitcast_fusion
  5.0 0.1 copy-done.3
  5.1 0.2 copy-done.4
  5.3 0.9 copy_bitcast_fusion.2
  6.2 202.5 %layer.1 = bf16[128,2048]{1,0:T(8,128)(2,1)} custom-call(f32[2]{0:T(128)} %lam_small.1, f32[2]{0:T(128)} %lam_large.1, bf16[2,1,512,128]{3,2,1,0:T(8,128)(2,1)} %get-tuple-element.8.k_small, bf16[2,1,512,128]{3,2,1,0:T(8,128)(2,1)} %get-tuple-element.7.v_small, bf16[2,1,512,128]{3,2,1,0:T(8,128)(2,1)} %get-tuple-element.6.q_small, ...), custom_call_target="tpu_custom_call" | custom-call | flops 60000002048 | bytes 16000000 | tf_op jit(solution)/shard_map/layer/pallas_call | solution.py:623
  208.7 1.9 copy.34
Async XLA Ops:
  1.3 1.0 copy-start
  3.1 1.0 copy-start.1
  3.1 1.0 copy-start.2
  4.1 0.9 copy-start.3
  4.1 1.2 copy-start.4

commit v3 on v2

--- a/solution.py
+++ b/solution.py
@@ -44,7 +44,8 @@
         self.small_size, self.large_size = small_size, large_size
         tiles = units // 128
         first = (tiles + 1) // 2 * 128
-        self.sizes, self.offsets = (first, units - first), (0, first)
+        self.sizes, self.offsets = (units - first, first), (0, units - first)
+        self.half_of = [(i + 1) // 2 % 2 for i in range(self.slots)]
         self.depth = features // n
         self.halves = max(1, self.depth // 128)
         self.span = self.depth // self.halves
@@ -59,13 +60,14 @@
             self.high //= 2
 
 
-def layer_kernel(plan, lam_small, lam_large, k_small, v_small, q_small, k_large, v_large, q_large, gain_ref,
+def layer_kernel(plan, lam_small, lam_large, k_small_in, v_small_in, q_small_in, k_large_in, v_large_in,
+                 q_large_in, gain_ref,
                  out_small, out_large, residual_ref, norm_ref, gate, up, down, out_ref,
-                 kv, q, o, att, pool, peak, total, acc, w_out, w_gate, w_up, w_down, x, hidden,
-                 send_half, got_half, send_sum, got_sum,
+                 k_small, v_small, q_small, k_large, v_large, q_large, kv, q, o, att, pool, peak, total, acc, w_out, w_gate, w_up, w_down, x, hidden,
                  kz_s, kz_r, vz_s, vz_r, qz_s, qz_r, kx_s, kx_r, vx_s, vx_r, loc, o_s, o_r,
                  wz_s, wz_r, wx_s, wx_r, own_w, wy_s, wy_r, wc_s, wc_r,
-                 ag_s, ag_r, agc_s, agc_r, rc_s, rc_r, r2_s, r2_r):
+                 ag_s, ag_r, agc_s, agc_r, rc_s, rc_r,
+                 ya_s, ya_r, zb_s, zb_r, za_s, za_r, yb_s, yb_r):
     slots, group, m, n = plan.slots, plan.group, plan.m, plan.n
     tokens, rows, chips, depth = plan.tokens, plan.rows, plan.chips, plan.depth
     features = plan.features
@@ -82,7 +84,8 @@
         if k == 2:
             large = jnp.logical_or(large, a == i)
     by_kind = ((1, jnp.logical_not(large)), (2, large))
-    by_parity = ((0, parity == 0), (1, parity == 1))
+    share = lax.rem((a + 1) // 2, 2)
+    by_parity = ((0, share == 0), (1, share == 1))
 
     def remote(src, dst, send, recv, sp, tp):
         return pltpu.make_async_remote_copy(
@@ -105,10 +108,20 @@
         send, recv = ((kz_s, kz_r), (vz_s, vz_r), (qz_s, qz_r))[what]
         return remote(source(i, what), dst, send.at[i], recv.at[a], i * group + b, t)
 
-    def to_self(i, what):
+    def keep(i, what):
         keys = pl.ds(0, plan.keys[i])
-        dst = (kv.at[keys, mine], kv.at[pl.ds(2, 1), mine], q.at[keys, a])[what]
-        return pltpu.make_async_copy(source(i, what), dst, loc.at[what])
+        if what == 0:
+            kv[keys, mine] = source(i, what)[...]
+        elif what == 1:
+            kv[pl.ds(2, 1), mine] = source(i, what)[...]
+        else:
+            q[keys, a] = source(i, what)[...]
+
+    def by_head(values, out):
+        width = out.shape[3]
+        for part in range(out.shape[1]):
+            piece = values[:, :, part * width : (part + 1) * width]
+            out[:, part] = jnp.transpose(piece, (1, 0, 2))
 
     def peer(j):
         return a * group + lax.rem(b + j, group)
@@ -116,6 +129,13 @@
     def k_x(k, i, j):
         part = kv.at[pl.ds(0, k), block_of(i)]
         return remote(part, part, kx_s.at[i, j - 1], kx_r.at[i, j - 1], peer(j), t)
+
+    def k_own(i, j):
+        keys = pl.ds(0, plan.keys[i])
+        return remote(source(i, 0), kv.at[keys, mine], kx_s.at[i, j - 1], kx_r.at[i, j - 1], peer(j), t)
+
+    def v_own(i, j):
+        return remote(source(i, 1), kv.at[pl.ds(2, 1), mine], vx_s.at[i, j - 1], vx_r.at[i, j - 1], peer(j), t)
 
     def v_x(i, j):
         part = kv.at[pl.ds(2, 1), block_of(i)]
@@ -144,7 +164,7 @@
                          pl.ds(pl.multiple_of(block * plan.span, plan.span), plan.span)]
 
     def w_z(k, i):
-        return remote(piece_in(k, i % 2), piece_at(k, i % 2, s), wz_s.at[k, i], wz_r.at[k, a],
+        return remote(piece_in(k, plan.half_of[i]), piece_at(k, plan.half_of[i], s), wz_s.at[k, i], wz_r.at[k, a],
                       i * group + b, t)
 
     def w_own(k, par):
@@ -154,10 +174,16 @@
         part = piece_at(k, par, i * group + b)
         return remote(part, part, wx_s.at[k, i, j - 1], wx_r.at[k, i, j - 1], peer(j), t)
 
-    def w_start(k):
+    def w_near(k):
+        for i in range(slots):
+            @pl.when(i == a + 1 - 2 * parity)
+            def _():
+                w_z(k, i).start()
+
+    def w_far(k):
         for distance in range(1, slots):
             for i in range(slots):
-                @pl.when(jnp.abs(a - i) == distance)
+                @pl.when(jnp.logical_and(jnp.abs(a - i) == distance, i != a + 1 - 2 * parity))
                 def _():
                     w_z(k, i).start()
 
@@ -172,17 +198,30 @@
                         for j in range(1, group):
                             w_x(k, par, i, j).start()
 
-    def w_forward(k):
+    def w_pass(k, par, i):
+        arrival(piece_at(k, par, i * group + b), wz_r.at[k, i])
+        for j in range(1, group):
+            w_x(k, par, i, j).start()
+
+    def pass_near(k):
+        for i in range(slots):
+            @pl.when(i == a + 1 - 2 * parity)
+            def _():
+                w_pass(k, plan.half_of[i ^ 1], i)
+
+    def pass_far(k):
         for par, when in by_parity:
             @pl.when(when)
             def _():
                 for distance in range(1, slots):
                     for i in range(slots):
-                        @pl.when(jnp.abs(a - i) == distance)
+                        @pl.when(jnp.logical_and(jnp.abs(a - i) == distance, i != a + 1 - 2 * parity))
                         def _():
-                            arrival(piece_at(k, par, i * group + b), wz_r.at[k, i])
-                            for j in range(1, group):
-                                w_x(k, par, i, j).start()
+                            w_pass(k, par, i)
+
+    def w_forward(k):
+        pass_near(k)
+        pass_far(k)
 
     def w_wait(k):
         for par, when in by_parity:
@@ -197,20 +236,28 @@
         return lax.rem(y + dy, chips) * 2 + c
 
     cut = out_small.shape[0]
-    spans = ((out_small, pl.ds(0, cut)), (out_large, pl.ds(cut, out_large.shape[0])))
+    deep = cut + out_large.shape[0]
+    spans = ((out_small, 0, cut), (out_large, cut, out_large.shape[0]))
+
+    def wo_at(tp, e):
+        return w_out.at[pl.ds(pl.multiple_of(tp * deep + spans[e][1], 128), spans[e][2])]
+
+    def stash(which, h, r, start, size):
+        low = features // plan.halves
+        return w_out.at[pl.ds((which * m + r) * rows, rows), pl.ds(h * low + start, size)]
+
 
     def wo_y(dy, e):
-        part, place = spans[e]
-        return remote(part, w_out.at[t, place], wy_s.at[dy - 1, e], wy_r.at[chips - dy - 1, e], s, tp_of(dy))
+        part = spans[e][0]
+        return remote(part, wo_at(t, e), wy_s.at[dy - 1, e], wy_r.at[chips - dy - 1, e], s, tp_of(dy))
 
     def wo_c(dy, e):
-        part, place = spans[e]
-        there = w_out.at[tp_of(dy), place]
+        part = spans[e][0]
+        there = wo_at(tp_of(dy), e)
         return remote(part if dy == 0 else there, there, wc_s.at[dy, e], wc_r.at[dy, e], s, partner)
 
     def wo_own(e):
-        part, place = spans[e]
-        return pltpu.make_async_copy(part, w_out.at[t, place], loc.at[3 + e])
+        return pltpu.make_async_copy(spans[e][0], wo_at(t, e), loc.at[e])
 
     pair = (a + 1 - 2 * parity) * group + b
 
@@ -225,16 +272,29 @@
     def row_near(r):
         return remote(x.at[r, 0], x.at[r, 1], agc_s.at[r], agc_r.at[r], s, partner)
 
+    side = features // plan.halves // 2
+
     def half_near(h, r):
-        return remote(send_half.at[h, r], got_half.at[h, r], rc_s.at[h, r], rc_r.at[h, r], s, partner)
-
-    def sum_y(h, dz, dy):
-        into = dz * chips + chips - dy
-        r = dz * chips + dy
-        return remote(send_sum.at[h, r], got_sum.at[h, into], r2_s.at[h, r], r2_r.at[h, into], s, tp_of(dy))
-
-    def sum_z(h):
-        return remote(send_sum.at[h, chips], got_sum.at[h, 0], r2_s.at[h, 0], r2_r.at[h, 0], pair, t)
+        return remote(stash(0, h, r, 0, 2 * side), stash(1, h, r, 0, 2 * side), rc_s.at[h, r], rc_r.at[h, r], s, partner)
+
+    by_y, by_z = (0, side), (side, side)
+
+    def y_first(h, dz, dy):
+        r, into = dz * chips + dy, dz * chips + chips - dy
+        return remote(stash(2, h, r, *by_y), stash(3, h, into, *by_y),
+                      ya_s.at[h, r], ya_r.at[h, into], s, tp_of(dy))
+
+    def z_second(h):
+        return remote(stash(2, h, chips, *by_y), stash(3, h, 0, *by_y),
+                      zb_s.at[h], zb_r.at[h], pair, t)
+
+    def z_first(h, dy):
+        return remote(stash(2, h, chips + dy, *by_z), stash(3, h, chips + dy, *by_z),
+                      za_s.at[h, dy], za_r.at[h, dy], pair, t)
+
+    def y_second(h, dy):
+        return remote(stash(2, h, dy, *by_z), stash(3, h, chips - dy, *by_z),
+                      yb_s.at[h, dy], yb_r.at[h, chips - dy], s, tp_of(dy))
 
     barrier = pltpu.get_barrier_semaphore()
     for i in range(slots):
@@ -245,11 +305,8 @@
                                     device_id_type=MESH)
     for j in range(1, group):
         pl.semaphore_signal(barrier, inc=1, device_id={"sp": peer(j), "tp": t}, device_id_type=MESH)
-    for i in range(slots):
-        @pl.when(a == i)
-        def _():
-            for what in range(3):
-                to_self(i, what).start()
+    by_head(k_large_in, k_large)
+    by_head(k_small_in, k_small)
     for e in range(2):
         wo_own(e).start()
     for par, when in by_parity:
@@ -257,6 +314,8 @@
         def _():
             for k in range(pieces):
                 w_own(k, par).start()
+    by_head(v_large_in, v_large)
+    by_head(v_small_in, v_small)
     pl.semaphore_wait(barrier, slots * m - 1 + group - 1)
 
     for what in range(3):
@@ -265,29 +324,31 @@
                 @pl.when(jnp.abs(a - i) == distance)
                 def _():
                     to_slot(i, what).start()
-    w_start(0)
+        if what == 1:
+            by_head(q_large_in, q_large)
+            by_head(q_small_in, q_small)
     for e in range(2):
         for dy in range(1, chips):
             wo_y(dy, e).start()
         wo_c(0, e).start()
-    if plan.sizes[1] < plan.sizes[0]:
-        @pl.when(parity == 1)
+    spare_units = plan.sizes[1] - plan.sizes[0]
+    if spare_units:
+        @pl.when(share == 0)
         def _():
-            spare = pl.ds(plan.sizes[1], plan.sizes[0] - plan.sizes[1])
-            w_gate[:, spare] = jnp.zeros((features, plan.sizes[0] - plan.sizes[1]), w_gate.dtype)
-            w_up[:, spare] = jnp.zeros((features, plan.sizes[0] - plan.sizes[1]), w_up.dtype)
+            spare = pl.ds(plan.sizes[0], spare_units)
+            w_gate[:, spare] = jnp.zeros((features, spare_units), w_gate.dtype)
+            w_up[:, spare] = jnp.zeros((features, spare_units), w_up.dtype)
             for h in range(plan.halves):
-                w_down[h, spare, :] = jnp.zeros(
-                    (plan.sizes[0] - plan.sizes[1], features // plan.halves), w_down.dtype)
+                w_down[h, spare, :] = jnp.zeros((spare_units, features // plan.halves), w_down.dtype)
 
     for i in range(slots):
         @pl.when(a == i)
         def _():
             for what in range(3):
-                to_self(i, what).wait()
+                keep(i, what)
             for j in range(1, group):
-                k_x(plan.keys[i], i, j).start()
-                v_x(i, j).start()
+                k_own(i, j).start()
+                v_own(i, j).start()
 
     for distance in range(1, slots):
         for i in range(slots):
@@ -305,8 +366,8 @@
                 for j in range(1, group):
                     v_x(i, j).start()
 
-    w_start(1)
-    w_start(2)
+    w_near(0)
+    w_far(0)
     for k in range(pieces):
         w_share(k)
 
@@ -411,8 +472,7 @@
     def wo_forward():
         for dy in range(1, chips):
             for e in range(2):
-                place = spans[e][1]
-                arrival(w_out.at[tp_of(dy), place], wy_r.at[dy - 1, e])
+                arrival(wo_at(tp_of(dy), e), wy_r.at[dy - 1, e])
                 wo_c(dy, e).start()
 
     def step_body(i, carry):
@@ -420,6 +480,13 @@
             @pl.when(i == at)
             def _():
                 ready(at)
+                if at == slots // 2 - 1:
+                    for k in (1, 2):
+                        w_near(k)
+                        w_far(k)
+                if at == slots // 2:
+                    for k in range(3, pieces):
+                        w_near(k)
         lax.fori_loop(0, parts, lambda part, c: attend(i, part) or c, 0)
 
         @pl.when(i > 0)
@@ -431,8 +498,7 @@
     lax.fori_loop(0, slots, step_body, 0)
     att[head] = o[a, pl.ds(pl.multiple_of(t * rows, rows), rows)]
     send(slots - 1)
-    w_start(3)
-    w_start(4)
+    w_far(3)
     w_forward(0)
     wo_forward()
     w_forward(1)
@@ -441,11 +507,14 @@
         wo_own(e).wait()
         for dy in range(chips):
             block = lax.rem(y + dy, chips) * 2 + 1 - c
-            arrival(w_out.at[block, spans[e][1]], wc_r.at[dy, e])
+            arrival(wo_at(block, e), wc_r.at[dy, e])
     for h in range(m * slots):
         @pl.when(head != h)
         def _():
             arrival(att.at[h], o_r.at[h])
+    for e in range(2):
+        for dy in range(chips):
+            wo_c(dy, e).wait_send()
     stretch = 512
     base = plan.features
     for start in range(0, features, stretch):
@@ -453,7 +522,7 @@
         sums = None
         for tt in range(m):
             left = jnp.concatenate([att[tt * slots + i] for i in plan.natural], axis=1)
-            term = jnp.dot(left, w_out[tt, :, cols], preferred_element_type=jnp.float32)
+            term = jnp.dot(left, w_out[pl.ds(tt * deep, deep), cols], preferred_element_type=jnp.float32)
             sums = term if sums is None else sums + term
         pool[1, pl.ds(0, rows), pl.ds(base + start, stretch)] = (
             residual_scale * residual_ref[:, cols].astype(jnp.float32) + sums)
@@ -463,25 +532,10 @@
     for dy in range(1, chips):
         row_y(0, dy).start()
     row_near(0).start()
-    for k in range(5, pieces):
-        w_start(k)
-    for k in range(2, plan.ups):
-        w_forward(k)
-    arrival(x.at[chips, 0], ag_r.at[chips])
-    for dy in range(1, chips):
-        row_y(1, dy).start()
-    row_near(chips).start()
-    w_forward(plan.ups)
-    for dz in range(2):
-        for dy in range(1, chips):
-            r = dz * chips + dy
-            arrival(x.at[r, 0], ag_r.at[r])
-            row_near(r).start()
-    w_forward(plan.ups + 1)
-    for r in range(peers):
-        arrival(x.at[r, 1], agc_r.at[r])
-
-    def gate_up(j):
+    for k in range(4, pieces):
+        w_far(k)
+
+    def gate_up(j, lo, hi):
         start, widths = plan.columns[j]
         cols = pl.ds(start, max(widths))
 
@@ -492,16 +546,61 @@
             hidden[r, :, cols] = (g / (1.0 + jnp.exp(-g)) * u).astype(hidden.dtype)
             return carry
 
-        lax.fori_loop(0, peers, one, 0)
-
-    done = plan.ups + 2
-    for j in range(len(plan.columns)):
+        lax.fori_loop(lo, hi, one, 0)
+
+    def forward_to(last):
+        for k in range(state["done"], min(last, pieces)):
+            if k < 3:
+                pass_near(k)
+            pass_far(k)
+            state["done"] = k + 1
+
+    def rows_y(dz):
+        for dy in range(1, chips):
+            r = dz * chips + dy
+            arrival(x.at[r, 0], ag_r.at[r])
+            row_near(r).start()
+
+    def rows_near(dz):
+        for r in range(dz * chips, dz * chips + chips):
+            arrival(x.at[r, 1], agc_r.at[r])
+
+    def columns_here(j):
         w_wait(2 * j)
         w_wait(2 * j + 1)
-        gate_up(j)
-        if done < pieces and j + 1 < len(plan.columns):
-            w_forward(done)
-            done += 1
+
+    state = {"done": 2}
+    ups = plan.ups
+    early = len(plan.columns) - 1
+    forward_to(3)
+    for k in range(3, pieces):
+        pass_near(k)
+    forward_to(4)
+    rows_y(0)
+    forward_to(5)
+    arrival(x.at[chips, 0], ag_r.at[chips])
+    for dy in range(1, chips):
+        row_y(1, dy).start()
+    row_near(chips).start()
+    rows_near(0)
+    for j in range(early):
+        forward_to(2 * j + 2)
+        columns_here(j)
+        gate_up(j, 0, chips)
+    forward_to(ups)
+    rows_y(1)
+    forward_to(ups + 1)
+    rows_near(1)
+    gate_up(0, chips, peers)
+    forward_to(ups + 2)
+    if early > 1:
+        gate_up(1, chips, peers)
+    forward_to(ups + 3)
+    for j in range(2, early):
+        gate_up(j, chips, peers)
+    columns_here(early)
+    gate_up(early, 0, peers)
+    forward_to(ups + 4)
 
     low = features // plan.halves
     band = min(512, low)
@@ -515,38 +614,60 @@
             cols = pl.ds(start, band)
             part = jnp.dot(hidden[r], w_down[h, :, cols], preferred_element_type=jnp.float32)
             kept(r, pl.ds(h * low + start, band))[...] = part[:rows]
-            send_half[h, r, :, cols] = part[rows:].astype(send_half.dtype)
-
-    def near_sum(h, r):
-        arrival(got_half.at[h, r], rc_r.at[h, r])
-        return kept(r, pl.ds(h * low, low))[...] + got_half[h, r].astype(jnp.float32)
+            stash(0, h, r, start, band)[...] = part[rows:].astype(w_out.dtype)
+
+    def chip_sum(h, r, which):
+        cols = pl.ds(h * low + which * side, side)
+        return kept(r, cols)[...] + stash(1, h, r, which * side, side)[...].astype(jnp.float32)
 
     def down_half(h):
-        order = [dz * chips + dy for dz in (1, 0) for dy in list(range(1, chips)) + [0]]
-        for r in order:
+        order = [chips + dy for dy in range(1, chips)] + [chips] + list(range(1, chips)) + [0]
+
+        def pass_on(r):
+            dz, dy = r // chips, r % chips
+            arrival(stash(1, h, r, 0, 2 * side), rc_r.at[h, r])
+            if dy:
+                stash(2, h, r, *by_y)[...] = chip_sum(h, r, 0).astype(w_out.dtype)
+                y_first(h, dz, dy).start()
+            if dz:
+                stash(2, h, r, *by_z)[...] = chip_sum(h, r, 1).astype(w_out.dtype)
+                z_first(h, dy).start()
+
+        for place, r in enumerate(order):
             down_rows(h, r)
             half_near(h, r).start()
-        for r in order:
-            if r % chips:
-                send_sum[h, r] = near_sum(h, r).astype(send_sum.dtype)
-                sum_y(h, r // chips, r % chips).start()
+            if place:
+                pass_on(order[place - 1])
+        pass_on(0)
 
     def plane_sum(h, dz):
-        result = near_sum(h, dz * chips)
+        result = chip_sum(h, dz * chips, 0)
         for dy in range(1, chips):
             r = dz * chips + dy
-            arrival(got_sum.at[h, r], r2_r.at[h, r])
-            result += got_sum[h, r].astype(jnp.float32)
+            arrival(stash(3, h, r, *by_y), ya_r.at[h, r])
+            result += stash(3, h, r, *by_y)[...].astype(jnp.float32)
         return result
 
-    def pass_pair(h):
-        send_sum[h, chips] = plane_sum(h, 1).astype(send_sum.dtype)
-        sum_z(h).start()
+    def line_sum(h, dy):
+        arrival(stash(3, h, chips + dy, *by_z), za_r.at[h, dy])
+        return chip_sum(h, dy, 1) + stash(3, h, chips + dy, *by_z)[...].astype(jnp.float32)
+
+    def second_sums(h):
+        stash(2, h, chips, *by_y)[...] = plane_sum(h, 1).astype(w_out.dtype)
+        z_second(h).start()
+        for dy in range(1, chips):
+            stash(2, h, dy, *by_z)[...] = line_sum(h, dy).astype(w_out.dtype)
+            y_second(h, dy).start()
 
     def finish(h):
-        result = plane_sum(h, 0)
-        arrival(got_sum.at[h, 0], r2_r.at[h, 0])
-        result += got_sum[h, 0].astype(jnp.float32)
+        first = plane_sum(h, 0)
+        arrival(stash(3, h, 0, *by_y), zb_r.at[h])
+        first += stash(3, h, 0, *by_y)[...].astype(jnp.float32)
+        second = line_sum(h, 0)
+        for dy in range(1, chips):
+            arrival(stash(3, h, dy, *by_z), yb_r.at[h, dy])
+            second += stash(3, h, dy, *by_z)[...].astype(jnp.float32)
+        result = jnp.concatenate([first, second], axis=1)
         for block in range(n):
             cols = pl.ds(block * depth + h * plan.span, plan.span)
             out_ref[:, cols] = (
@@ -556,15 +677,13 @@
 
     for h in range(plan.halves):
         first = plan.ups + 2 * h
-        for k in range(done, first + 2):
-            w_forward(k)
-        done = max(done, first + 2)
+        forward_to(first + 2)
         w_wait(first)
         w_wait(first + 1)
-        if h > 0:
-            pass_pair(h - 1)
         down_half(h)
-    pass_pair(plan.halves - 1)
+        if h:
+            second_sums(h - 1)
+    second_sums(plan.halves - 1)
     for h in range(plan.halves):
         finish(h)
 
@@ -595,25 +714,27 @@
     for e in range(2):
         for dy in range(1, chips):
             wo_y(dy, e).wait_send()
-        for dy in range(chips):
-            wo_c(dy, e).wait_send()
     row_z().wait_send()
     for r in range(peers):
         row_near(r).wait_send()
         for h in range(plan.halves):
             half_near(h, r).wait_send()
+            if r % chips:
+                y_first(h, r // chips, r % chips).wait_send()
         if r % chips:
             row_y(r // chips, r % chips).wait_send()
-            for h in range(plan.halves):
-                sum_y(h, r // chips, r % chips).wait_send()
     for h in range(plan.halves):
-        sum_z(h).wait_send()
+        z_second(h).wait_send()
+        for dy in range(chips):
+            z_first(h, dy).wait_send()
+            if dy:
+                y_second(h, dy).wait_send()
 
 
 def run_layer(plan, lams, small, large, gain, outs, residual, norm_gain, mixer, width):
     dma = pltpu.SemaphoreType.DMA
     slots, n, m, peers, chips = plan.slots, plan.n, plan.m, plan.peers, plan.chips
-    rows, features, units, halves = plan.rows, plan.features, plan.sizes[0], plan.halves
+    rows, features, units, halves = plan.rows, plan.features, plan.sizes[1], plan.halves
     high, pieces = plan.high, len(plan.pieces)
     anywhere = pl.BlockSpec(memory_space=pl.ANY)
     vmem = pl.BlockSpec(memory_space=pltpu.VMEM)
@@ -623,9 +744,15 @@
     return pl.pallas_call(
         functools.partial(layer_kernel, plan),
         out_shape=jax.ShapeDtypeStruct((rows, features), bf16),
-        in_specs=[smem] * 2 + [anywhere] * 6 + [vmem] + [anywhere] * 2 + [vmem] * 2 + [anywhere] * 3,
+        in_specs=[smem] * 2 + [vmem] * 7 + [anywhere] * 2 + [vmem] * 2 + [anywhere] * 3,
         out_specs=vmem,
         scratch_shapes=[
+            pltpu.VMEM((small[0].shape[1], 1, plan.tokens, width), bf16),
+            pltpu.VMEM((small[0].shape[1], 1, plan.tokens, width), bf16),
+            pltpu.VMEM((small[0].shape[1], 1, plan.tokens, width), bf16),
+            pltpu.VMEM((large[0].shape[1], 2, plan.tokens, width), bf16),
+            pltpu.VMEM((large[0].shape[1], 1, plan.tokens, width), bf16),
+            pltpu.VMEM((large[0].shape[1], 2, plan.tokens, width), bf16),
             pltpu.VMEM((3, n * plan.tokens, width), bf16),
             pltpu.VMEM((2, slots, plan.tokens, width), bf16),
             pltpu.VMEM((slots, plan.tokens, width), bf16),
@@ -634,23 +761,24 @@
             pltpu.VMEM((2, high, 128), f32),
             pltpu.VMEM((2, high, 128), f32),
             pltpu.VMEM((2, high, width), f32),
-            pltpu.VMEM((m, slots * width, features), bf16),
+            pltpu.VMEM((max(m * slots * width, 4 * m * rows), features), bf16),
             pltpu.VMEM((features, units), bf16),
             pltpu.VMEM((features, units), bf16),
             pltpu.VMEM((halves, units, features // halves), bf16),
             pltpu.VMEM((peers, 2, rows, features), bf16),
             pltpu.VMEM((peers, 2 * rows, units), bf16),
-        ] + [pltpu.VMEM((halves, peers, rows, features // halves), bf16)] * 4 + [
             dma((slots,)), dma((slots,)), dma((slots,)), dma((slots,)), dma((slots,)), dma((slots,)),
             dma((slots, others)), dma((slots, others)), dma((slots, others)), dma((slots, others)),
-            dma((5,)),
+            dma((2,)),
             dma((slots, plan.tokens // rows)), dma((m * slots,)),
             dma((pieces, slots)), dma((pieces, slots)),
             dma((pieces, slots, others)), dma((pieces, slots, others)),
             dma((pieces,)),
             dma((ahead, 2)), dma((ahead, 2)), dma((chips, 2)), dma((chips, 2)),
             dma((peers,)), dma((peers,)), dma((peers,)), dma((peers,)),
-            dma((halves, peers)), dma((halves, peers)), dma((halves, peers)), dma((halves, peers)),
+            dma((halves, peers)), dma((halves, peers)),
+            dma((halves, peers)), dma((halves, peers)), dma((halves,)), dma((halves,)),
+            dma((halves, chips)), dma((halves, chips)), dma((halves, chips)), dma((halves, chips)),
         ],
         compiler_params=pltpu.CompilerParams(
             vmem_limit_bytes=61 * 2**20, has_side_effects=True, collective_id=0),
@@ -677,12 +805,8 @@
     plan = Plan(n, m, heads_small, heads_large, tokens, rows, query_small.shape[2] // 2,
                 query_large.shape[2] // 2, features, gate_weight.shape[1])
 
-    def by_head(values):
-        parts = values.reshape(tokens, values.shape[1], -1, width)
-        return jnp.transpose(parts, (1, 2, 0, 3))
-
-    small = [by_head(v) for v in (key_small, value_small, query_small)]
-    large = [by_head(v) for v in (key_large, value_large, query_large)]
+    small = (key_small, value_small, query_small)
+    large = (key_large, value_large, query_large)
     return run_layer(
         plan, (lambda_small, lambda_large), small, large, head_gain, (output_small, output_large),
         residual, norm_gain, (gate_weight, up_weight, down_weight), width)

time: 211 us -> 197 us (0.934)
  Pallas kernels: 203 us -> 193 us
  local copies, waits for them, and re-layouts: 8.04 us -> 1.88 us
    pallas_call x1, Pallas kernels: 203 us -> 193 us  [run_layer(): pl.pallas_call(functools.partial(layer_kernel, plan), out_shape=jax.Shape...]
    unnamed x13 -> x1, local copies, waits for them, and re-layouts: 4.3 us -> 1.88 us
where the time goes in v3:
time: 197 us; the launch traced here: 195 us
  Pallas kernels  193 us (98%)
    pallas_call x1, Pallas kernels, run_layer(): pl.pallas_call(functools.partial(layer_kernel, plan), out_shape=jax.Shape...  193 us

profile of v3, /device:TPU:0, one launch (start us, length us, event | category | flops | bytes accessed | tf_op | source)
XLA Modules:
  0.0 194.8 jit_solution(362594809459384201)
XLA Ops:
  0.0 193.0 %layer.1 = bf16[128,2048]{1,0:T(8,128)(2,1)} custom-call(f32[2]{0:T(128)} %lam_small.1, f32[2]{0:T(128)} %lam_large.1, bf16[512,2,128]{2,1,0:T(2,128)(2,1)} %k_small_in.1, bf16[512,2,128]{2,1,0:T(2,128)(2,1)} %v_small_in.1, bf16[512,2,128]{2,1,0:T(2,128)(2,1)} %q_small_in.1, bf16[512,2,256]{2,1,0:T(2,128)(2,1)} %k_large_in.1, ...), custom_call_target="tpu_custom_call" | custom-call | flops 60000002048 | bytes 16000000 | tf_op jit(solution)/shard_map/layer/pallas_call | solution.py:744
  193.0 1.9 copy.18

commit v4 on v3

--- a/solution.py
+++ b/solution.py
@@ -485,7 +485,7 @@
                         w_near(k)
                         w_far(k)
                 if at == slots // 2:
-                    for k in range(3, pieces):
+                    for k in (3, 4):
                         w_near(k)
         lax.fori_loop(0, parts, lambda part, c: attend(i, part) or c, 0)
 
@@ -499,6 +499,9 @@
     att[head] = o[a, pl.ds(pl.multiple_of(t * rows, rows), rows)]
     send(slots - 1)
     w_far(3)
+    for k in range(5, pieces):
+        w_near(k)
+    w_far(4)
     w_forward(0)
     wo_forward()
     w_forward(1)
@@ -532,7 +535,7 @@
     for dy in range(1, chips):
         row_y(0, dy).start()
     row_near(0).start()
-    for k in range(4, pieces):
+    for k in range(5, pieces):
         w_far(k)
 
     def gate_up(j, lo, hi):
@@ -582,6 +585,25 @@
     for dy in range(1, chips):
         row_y(1, dy).start()
     row_near(chips).start()
+    for i in range(slots):
+        @pl.when(a != i)
+        def _():
+            for what in range(3):
+                to_slot(i, what).wait_send()
+
+        for kind, when in by_kind:
+            @pl.when(when)
+            def _():
+                for j in range(1, group):
+                    k_x(kind, i, j).wait_send()
+                    v_x(i, j).wait_send()
+        for which in range(tokens // rows):
+            @pl.when(jnp.logical_not(jnp.logical_and(i == a, which == t)))
+            def _():
+                o_copy(i, which).wait_send()
+    for e in range(2):
+        for dy in range(1, chips):
+            wo_y(dy, e).wait_send()
     rows_near(0)
     for j in range(early):
         forward_to(2 * j + 2)
@@ -684,36 +706,21 @@
         if h:
             second_sums(h - 1)
     second_sums(plan.halves - 1)
-    for h in range(plan.halves):
-        finish(h)
-
     for i in range(slots):
         @pl.when(a != i)
         def _():
-            for what in range(3):
-                to_slot(i, what).wait_send()
             for k in range(pieces):
                 w_z(k, i).wait_send()
 
-        for k, when in by_kind:
-            @pl.when(when)
-            def _():
-                for j in range(1, group):
-                    k_x(k, i, j).wait_send()
-                    v_x(i, j).wait_send()
         for par, when in by_parity:
             @pl.when(when)
             def _():
                 for j in range(1, group):
                     for k in range(pieces):
                         w_x(k, par, i, j).wait_send()
-        for which in range(tokens // rows):
-            @pl.when(jnp.logical_not(jnp.logical_and(i == a, which == t)))
-            def _():
-                o_copy(i, which).wait_send()
-    for e in range(2):
-        for dy in range(1, chips):
-            wo_y(dy, e).wait_send()
+    for h in range(plan.halves):
+        finish(h)
+
     row_z().wait_send()
     for r in range(peers):
         row_near(r).wait_send()

time: 197 us -> 186 us (0.944)
  Pallas kernels: 193 us -> 184 us
    pallas_call x1, Pallas kernels: 193 us -> 184 us  [run_layer(): pl.pallas_call(functools.partial(layer_kernel, plan), out_shape=jax.Shape...]
where the time goes in v4:
time: 186 us
  Pallas kernels  184 us (99%)
  local copies, waits for them, and re-layouts  1.88 us (1%)
    pallas_call x1, Pallas kernels, run_layer(): pl.pallas_call(functools.partial(layer_kernel, plan), out_shape=jax.Shape...  184 us

profile of v4, /device:TPU:0, one launch (start us, length us, event | category | flops | bytes accessed | tf_op | source)
XLA Modules:
  0.0 185.6 jit_solution(11731759216880542526)
XLA Ops:
  0.0 183.7 %layer.1 = bf16[128,2048]{1,0:T(8,128)(2,1)} custom-call(f32[2]{0:T(128)} %lam_small.1, f32[2]{0:T(128)} %lam_large.1, bf16[512,2,128]{2,1,0:T(2,128)(2,1)} %k_small_in.1, bf16[512,2,128]{2,1,0:T(2,128)(2,1)} %v_small_in.1, bf16[512,2,128]{2,1,0:T(2,128)(2,1)} %q_small_in.1, bf16[512,2,256]{2,1,0:T(2,128)(2,1)} %k_large_in.1, ...), custom_call_target="tpu_custom_call" | custom-call | flops 60000002048 | bytes 16000000 | tf_op jit(solution)/shard_map/layer/pallas_call | solution.py:751
  183.7 1.9 %copy.18 = bf16[128,2048]{1,0:T(8,128)(2,1)} copy(bf16[128,2048]{1,0:T(8,128)(2,1)} %layer.1) | data formatting | bytes 1048576
